TPU v7x, 512 devices: a whole 4x8x8 slice. The times are simulated.
512 devices in a mesh: rep: 2 (over z_hi), fs: 32 (over z_lo, y), tp: 8 (over x, core).
Axes of the slice: x: 4, y: 8, z: 8 (z_hi: 2, z_lo: 4; z = z_hi * 4 + z_lo), core: 2. Of those that a mesh axis runs over, the one named last changes fastest.
Arguments:
- tokens: bfloat16 [24576, 2048], P(('rep', 'fs'), 'tp'), may hold values from -6 to 6
- mixing_norm_gain: float32 [2048], replicated, may hold values from 0.1 to 1.9
- recurrent_input_weight: float32 [2048, 3072], P('fs', 'tp'), may hold values from -0.125 to 0.125
- recurrent_input_scale: float32 [3072], P('tp'), may hold values from 0.5 to 2
- convolution_kernel_taps: float32 [4, 3072], P(None, 'tp'), may hold values from -3 to 3
- recurrence_gate_weight_blocks: bfloat16 [24, 128, 128], P('tp'), may hold values from -0.5 to 0.5
- input_gate_weight_blocks: bfloat16 [24, 128, 128], P('tp'), may hold values from -0.5 to 0.5
- channel_decay_parameter: float32 [3072], P('tp'), may hold values from 3 to 9
- token_extra_log_decay: float32 [24576], P(('rep', 'fs')), may hold values from -0.7 to 0
- mixing_output_weight: float32 [3072, 2048], P('tp', 'fs'), may hold values from -0.109375 to 0.109375
- mixing_output_scale: float32 [2048], P('fs'), may hold values from 0.5 to 2
- feedforward_norm_gain: float32 [2048], replicated, may hold values from 0.1 to 1.9
- feedforward_gate_weight: float32 [2048, 5120], P('fs', 'tp'), may hold values from -0.125 to 0.125
- feedforward_gate_scale: float32 [5120], P('tp'), may hold values from 0.5 to 2
- feedforward_up_weight: float32 [2048, 5120], P('fs', 'tp'), may hold values from -0.125 to 0.125
- feedforward_up_scale: float32 [5120], P('tp'), may hold values from 0.5 to 2
- feedforward_down_weight: float32 [5120, 2048], P('tp', 'fs'), may hold values from -0.078125 to 0.078125
- feedforward_down_scale: float32 [2048], P('fs'), may hold values from 0.5 to 2
Outputs:
- layer_out: bfloat16 [24576, 2048], P(('rep', 'fs'), 'tp')
All inputs are finite; a program needn't handle non-finite values.
Results may differ from a plain program's by a relative error of at most 0.02.
Values may be sent and summed in bfloat16 or wider, within the bound.
No kernel may reach another device: no remote copies, remote signals or barrier semaphores. Data moves between devices by JAX's collectives and lax.ppermute only.
A program may use at most 64 MiB of HBM per device.

v0:
```python
import jax
import jax.numpy as jnp
from jax import lax
from jax.experimental import pallas as pl
from jax.experimental.pallas import tpu as pltpu
from jax.sharding import Mesh
from jax.sharding import PartitionSpec as P

FS = ("z", "y")
TP = ("x", "c")
REP_FS = ("rep", "z", "y")
EPS = 1e-06
DECAY_FACTOR = 8.0
CHUNKS = 8
F32 = jnp.float32
BF16 = jnp.bfloat16


def shift_z(value, step):
    count = lax.axis_size("rep") * lax.axis_size("z")
    return lax.ppermute(value, ("rep", "z"), [(i, (i + step) % count) for i in range(count)])


def swap(value, axis):
    return lax.all_to_all(value, axis, split_axis=0, concat_axis=0, tiled=True)


def copies_to(value, axis):
    return swap(jnp.broadcast_to(value, (lax.axis_size(axis), *value.shape)), axis)


def to_partner(value):
    return lax.ppermute(value, "c", [(0, 1), (1, 0)])


def chips_in_order(block):
    return copies_to(block, "x")


def share_sums(kept, sent):
    pair = (kept.astype(F32) + to_partner(sent).astype(F32)).astype(BF16)
    return swap(pair, "x").astype(F32).sum(axis=0)


def over_z(own):
    before = shift_z(own, 1)
    after = shift_z(own, -1)
    half = own.shape[0] // 2
    far_low = shift_z(after[:half], -1)
    far_high = shift_z(before[half:], 1)
    return own, before, after, far_low, far_high


def over_y(piece):
    return copies_to(piece, "y").reshape(-1, piece.shape[1])


def gather(piece, axes):
    return lax.all_gather(piece, axes, axis=0, tiled=True)


def z_then_y(piece):
    near = (piece, shift_z(piece, 1), shift_z(piece, -1), shift_z(piece, 2))
    joined = jnp.concatenate(near, axis=1)
    return gather(joined, "y")


def dot(a, b):
    return jnp.dot(a, b, preferred_element_type=F32)


def dot_t(a, b):
    return lax.dot_general(a, b, (((1,), (1,)), ((), ())), preferred_element_type=F32)


def normalize(blocks, gain_ref, normed_ref):
    total = None
    for block, _, _ in blocks:
        v = block[...].astype(F32)
        part = jnp.sum(v * v, axis=-1, keepdims=True)
        total = part if total is None else total + part
    inverse = lax.rsqrt(total / (len(blocks) * blocks[0][0].shape[1]) + EPS)
    for block, x, c in blocks:
        v = block[...].astype(F32)
        normed_ref[x, c] = (v * inverse * gain_ref[x, c]).astype(BF16)


def halves(normed_ref, chip):
    return jnp.concatenate([normed_ref[chip, 0], normed_ref[chip, 1]], axis=1)


def recurrence_kernel(
    place_ref,
    rows_ref,
    partner_ref,
    gain_ref,
    own_ref,
    before_ref,
    after_ref,
    far_low_ref,
    far_high_ref,
    scale_ref,
    taps_ref,
    recur_ref,
    input_ref,
    rate_ref,
    extra_ref,
    kept_ref,
    sent_ref,
    normed_ref,
    padded_ref,
    decay_ref,
    value_ref,
):
    rows = rows_ref.shape[1]
    width = scale_ref.shape[1]
    core = place_ref[0]
    own, before, after, far = (place_ref[i] for i in range(1, 5))
    blocks = [(rows_ref.at[i], i, core) for i in range(rows_ref.shape[0])]
    blocks += [(partner_ref.at[i], i, 1 - core) for i in range(rows_ref.shape[0])]
    normalize(blocks, gain_ref, normed_ref)
    total = dot(halves(normed_ref, own), own_ref[:, :width])
    total += dot(halves(normed_ref, before), before_ref[:, :width])
    total += dot(halves(normed_ref, after), after_ref[:, :width])
    total += dot(normed_ref[far, 0], far_low_ref[:, :width])
    total += dot(normed_ref[far, 1], far_high_ref[:, :width])
    taps = taps_ref.shape[0]
    padded_ref[0:8, :] = jnp.zeros((8, width), F32)
    padded_ref[8:, :] = (total * scale_ref[...]).astype(BF16).astype(F32)
    conv = None
    for k in range(taps):
        start = 8 - (taps - 1) + k
        term = taps_ref[k : k + 1, :] * padded_ref[start : start + rows, :]
        conv = term if conv is None else conv + term
    low = conv.astype(BF16)
    size = recur_ref.shape[1]
    for n in range(recur_ref.shape[0]):
        cols = slice(n * size, (n + 1) * size)
        gate = jax.nn.sigmoid(dot(low[:, cols], recur_ref[n]))
        chosen = jax.nn.sigmoid(dot(low[:, cols], input_ref[n]))
        logarithm = gate * rate_ref[:, cols] + extra_ref[...]
        decay = jnp.exp(logarithm)
        rest = jnp.tanh(-logarithm) * (1.0 + decay * decay)
        decay_ref[n] = decay
        value_ref[n] = jnp.sqrt(rest) * chosen * conv[:, cols]
    count = recur_ref.shape[0]
    steps = rows // CHUNKS

    def step(t, carry):
        new = []
        for n in range(count):
            at = (n, pl.ds(t, CHUNKS, stride=steps), slice(None))
            decay = decay_ref[at]
            state = decay * carry[2 * n] + value_ref[at]
            product = decay * carry[2 * n + 1]
            value_ref[at] = state
            decay_ref[at] = product
            new += [state, product]
        return tuple(new)

    first = (jnp.zeros((CHUNKS, size), F32), jnp.ones((CHUNKS, size), F32)) * count
    ends = lax.fori_loop(0, steps, step, first, unroll=8)
    states = []
    for n in range(count):
        state, product = ends[2 * n], ends[2 * n + 1]
        enter = jnp.zeros((1, size), F32)
        pieces = []
        for chunk in range(CHUNKS):
            span = slice(chunk * steps, (chunk + 1) * steps)
            pieces.append((value_ref[n, span, :] + decay_ref[n, span, :] * enter).astype(BF16))
            enter = state[chunk : chunk + 1] + product[chunk : chunk + 1] * enter
        states.append(jnp.concatenate(pieces, axis=0))
    low = jnp.concatenate(states, axis=1)
    outs = (core, kept_ref, sent_ref)
    store(outs, own, dot_t(low, own_ref[:, width:]))
    store(outs, before, dot_t(low, before_ref[:, width:]))
    store(outs, after, dot_t(low, after_ref[:, width:]))
    low_part = dot_t(low, far_low_ref[:, width:])
    high_part = dot_t(low, far_high_ref[:, width:])
    store(outs, far, jnp.concatenate([low_part, high_part], axis=1))


def store(outs, place, product):
    core, kept_ref, sent_ref = outs
    width = kept_ref.shape[2]
    first = product[:, :width].astype(BF16)
    second = product[:, width:].astype(BF16)
    kept_ref[place] = jnp.where(core == 0, first, second)
    sent_ref[place] = jnp.where(core == 0, second, first)


def ffn_kernel(
    place_ref,
    rows_ref,
    partner_ref,
    gain_ref,
    weights_ref,
    gate_scale_ref,
    up_scale_ref,
    kept_ref,
    sent_ref,
    normed_ref,
):
    core = place_ref[0]
    places = [place_ref[i] for i in range(1, 5)]
    blocks = [(rows_ref.at[i], i, core) for i in range(rows_ref.shape[0])]
    blocks += [(partner_ref.at[i], i, 1 - core) for i in range(rows_ref.shape[0])]
    normalize(blocks, gain_ref, normed_ref)
    width = gate_scale_ref.shape[1]
    total = None
    for k in range(4):
        start = 3 * k * width
        part = dot(halves(normed_ref, places[k]), weights_ref[:, start : start + 2 * width])
        total = part if total is None else total + part
    gate = total[:, :width] * gate_scale_ref[...]
    up = total[:, width:] * up_scale_ref[...]
    hidden = (gate * jax.nn.sigmoid(gate) * up).astype(BF16)
    outs = (core, kept_ref, sent_ref)
    for k in range(4):
        start = (3 * k + 2) * width
        store(outs, places[k], dot_t(hidden, weights_ref[:, start : start + width]))


def call(kernel, place, args, rows, width, scratch, flops):
    vmem = pl.BlockSpec(memory_space=pltpu.VMEM)
    return pl.pallas_call(
        kernel,
        out_shape=[jax.ShapeDtypeStruct((4, rows, width), BF16)] * 2,
        in_specs=[pl.BlockSpec(memory_space=pltpu.SMEM)] + [vmem] * len(args),
        out_specs=[vmem, vmem],
        scratch_shapes=[pltpu.VMEM((4, 2, rows, width), BF16)] + scratch,
        compiler_params=pltpu.CompilerParams(vmem_limit_bytes=56 * 1024 * 1024),
        cost_estimate=pl.CostEstimate(flops=flops, transcendentals=0, bytes_accessed=0),
    )(place, *args)


def layer(
    tokens,
    mixing_norm_gain,
    recurrent_input_weight,
    recurrent_input_scale,
    convolution_kernel_taps,
    recurrence_gate_weight_blocks,
    input_gate_weight_blocks,
    channel_decay_parameter,
    token_extra_log_decay,
    mixing_output_weight,
    mixing_output_scale,
    feedforward_norm_gain,
    feedforward_gate_weight,
    feedforward_gate_scale,
    feedforward_up_weight,
    feedforward_up_scale,
    feedforward_down_weight,
    feedforward_down_scale,
):
    rows, features = tokens.shape
    width = recurrent_input_weight.shape[1]
    z_count = lax.axis_size("z")
    z = lax.axis_index("z")
    near = jnp.array([0, 3, 1, 2], jnp.int32)
    place = jnp.concatenate([lax.axis_index("c")[None], (z + near) % z_count])

    mix_rows = (mixing_output_weight * mixing_output_scale).T
    mixing = jnp.concatenate([recurrent_input_weight, mix_rows], axis=1).astype(BF16)
    down = (feedforward_down_weight * feedforward_down_scale).T
    ffn = jnp.concatenate([feedforward_gate_weight, feedforward_up_weight, down], axis=1)
    ffn = ffn.astype(BF16)

    blocks = over_z(over_y(mixing))
    ffn_blocks = z_then_y(ffn)
    rate = -DECAY_FACTOR * jax.nn.softplus(-channel_decay_parameter)
    count, size = recurrence_gate_weight_blocks.shape[:2]
    tok = chips_in_order(tokens)
    mix_terms = call(
        recurrence_kernel,
        place,
        (
            tok,
            to_partner(tok),
            mixing_norm_gain.reshape(4, 2, 1, -1),
            *blocks,
            recurrent_input_scale.reshape(1, -1),
            convolution_kernel_taps,
            recurrence_gate_weight_blocks,
            input_gate_weight_blocks,
            rate.reshape(1, -1),
            token_extra_log_decay.reshape(-1, 1),
        ),
        rows,
        features,
        [
            pltpu.VMEM((rows + 8, width), F32),
            pltpu.VMEM((count, rows, size), F32),
            pltpu.VMEM((count, rows, size), F32),
        ],
        4 * rows * width * features * 8,
    )
    mixed = (tokens.astype(F32) + share_sums(*mix_terms)).astype(BF16)
    mid = chips_in_order(mixed)
    hidden_width = feedforward_gate_weight.shape[1]
    down_terms = call(
        ffn_kernel,
        place,
        (
            mid,
            to_partner(mid),
            feedforward_norm_gain.reshape(4, 2, 1, -1),
            ffn_blocks,
            feedforward_gate_scale.reshape(1, -1),
            feedforward_up_scale.reshape(1, -1),
        ),
        rows,
        features,
        [],
        6 * rows * hidden_width * features * 8,
    )
    return (mixed.astype(F32) + share_sums(*down_terms)).astype(BF16)


def solution(mesh):
    torus = Mesh(
        mesh.devices.reshape(mesh.shape["rep"], 4, 8, 4, 2), ("rep", "z", "y", "x", "c")
    )
    return jax.shard_map(
        layer,
        mesh=torus,
        in_specs=(
            P(REP_FS, TP),
            P(),
            P(FS, TP),
            P(TP),
            P(None, TP),
            P(TP, None, None),
            P(TP, None, None),
            P(TP),
            P(REP_FS),
            P(TP, FS),
            P(FS),
            P(),
            P(FS, TP),
            P(TP),
            P(FS, TP),
            P(TP),
            P(TP, FS),
            P(FS),
        ),
        out_specs=P(REP_FS, TP),
        check_vma=False,
    )
```

profile of v0, /device:TPU:1, one launch (start us, length us, event | category | flops | bytes accessed | tf_op | source)
XLA Modules:
  0.0 202.2 jit_solution(2478720204848910339)
XLA Ops:
  6.5 0.0 all-gather.2.cloned.1.call-start
  6.5 0.9 constant_dynamic-update-slice_fusion.5
  7.5 0.9 constant_dynamic-update-slice_fusion.4
  8.4 0.0 copy-start.8
  8.4 1.0 constant_dynamic-update-slice_fusion.3
  9.5 0.0 copy-start.9
  9.5 0.0 copy-start.15
  9.5 4.8 %collective-permute-start.7 = (bf16[64,1920]{1,0:T(8,128)(2,1)S(1)}, bf16[64,1920]{1,0:T(8,128)(2,1)S(1)}, u32[]{:S(2)}, u32[]{:S(2)}) collective-permute-start(bf16[64,1920]{1,0:T(8,128)(2,1)S(1)} %pad_maximum_fusion), channel_id=1, source_target_pairs={{0,64},{64,128},{128,192},{192,256},{256,320},{320,384},{384,448},... | collective-permute-start | bytes 737288 | tf_op jit(solution)/shard_map/ppermute | solution.py:21
  14.4 8.6 %collective-permute-start.8 = (bf16[64,1920]{1,0:T(8,128)(2,1)S(1)}, bf16[64,1920]{1,0:T(8,128)(2,1)S(1)}, u32[]{:S(2)}, u32[]{:S(2)}) collective-permute-start(bf16[64,1920]{1,0:T(8,128)(2,1)S(1)} %pad_maximum_fusion), channel_id=1, source_target_pairs={{0,448},{64,0},{128,64},{192,128},{256,192},{320,256},{384,320},{4... | collective-permute-start | bytes 737288 | tf_op jit(solution)/shard_map/ppermute | solution.py:21
  22.9 1.9 collective-permute-start.9
  24.9 1.8 collective-permute-done.7
  26.7 0.9 collective-permute-done.8
  27.6 11.2 %collective-permute-done.9 = bf16[64,1920]{1,0:T(8,128)(2,1)S(1)} collective-permute-done((bf16[64,1920]{1,0:T(8,128)(2,1)S(1)}, bf16[64,1920]{1,0:T(8,128)(2,1)S(1)}, u32[]{:S(2)}, u32[]{:S(2)}) %collective-permute-start.9) | collective-permute-done | bytes 245792 | tf_op jit(solution)/shard_map/ppermute | solution.py:21
  38.8 0.0 copy-start.4
  38.8 1.0 copy-done.4
  39.9 0.0 all-gather.2.cloned.1.call-update
  39.9 0.0 copy-start.6
  39.9 0.1 fusion.1
  40.0 0.1 broadcast_in_dim.16
  40.1 32.1 %all_to_all.25 = bf16[8,64,768]{2,1,0:T(8,128)(2,1)S(1)} all-to-all(bf16[8,64,768]{2,1,0:T(8,128)(2,1)S(1)} %broadcast_in_dim.16), channel_id=1, replica_groups=mesh['rep'=2,'z'=4,'y'=8,'x'=4,'c'=2] {'y'}, dimensions={0} | all-to-all | bytes 1572864 | tf_op jit(solution)/shard_map/all_to_all | solution.py:25
  72.2 1.0 broadcast_in_dim.15
  73.2 4.2 %all-to-all-start = ((bf16[4,384,256]{2,1,0:T(8,128)(2,1)}), bf16[4,384,256]{2,1,0:T(8,128)(2,1)S(1)}, u32[]{:S(2)}, u32[]{:S(2)}) async-start(bf16[4,384,256]{2,1,0:T(8,128)(2,1)} %broadcast_in_dim.15), calls=%async_computation | async-start | bytes 1572864 | tf_op jit(solution)/shard_map/all_to_all | solution.py:25
  77.4 1.9 collective-permute-start.2
  79.3 3.4 %collective-permute-start.1 = (bf16[512,768]{1,0:T(8,128)(2,1)S(1)}, bf16[512,768]{1,0:T(8,128)(2,1)S(1)}, u32[]{:S(2)}, u32[]{:S(2)}) collective-permute-start(bf16[512,768]{1,0:T(8,128)(2,1)S(1)} %bitcast.10), channel_id=1, source_target_pairs={{0,64},{64,128},{128,192},{192,256},{256,320},{320,384},{384,448},... | collective-permute-start | bytes 2359304 | tf_op jit(solution)/shard_map/ppermute | solution.py:21
  82.7 3.1 %all-to-all-done.rows_ref = bf16[4,384,256]{2,1,0:T(8,128)(2,1)S(1)} async-done(((bf16[4,384,256]{2,1,0:T(8,128)(2,1)}), bf16[4,384,256]{2,1,0:T(8,128)(2,1)S(1)}, u32[]{:S(2)}, u32[]{:S(2)}) %all-to-all-start) | async-done | bytes 786464 | tf_op jit(solution)/shard_map/all_to_all | solution.py:25
  85.8 9.1 %collective-permute-start = (bf16[4,384,256]{2,1,0:T(8,128)(2,1)S(1)}, bf16[4,384,256]{2,1,0:T(8,128)(2,1)}, u32[]{:S(2)}, u32[]{:S(2)}) collective-permute-start(bf16[4,384,256]{2,1,0:T(8,128)(2,1)S(1)} %all-to-all-done.rows_ref), channel_id=1, source_target_pairs={{0,1},{1,0},{2,3},{3,2},{4,5},{5,4},{6,7},{7,6},{8,9},{9,8},{10,11... | collective-permute-start | bytes 2359304 | tf_op jit(solution)/shard_map/ppermute | solution.py:33
  95.0 0.0 collective-permute-done.2.after_ref
  95.0 0.8 slice.8
  95.8 1.9 collective-permute-start.3
  97.8 0.0 collective-permute-done.1.before_ref
  97.8 0.0 copy-start.3
  97.8 3.4 %collective-permute-start.4 = (bf16[256,768]{1,0:T(8,128)(2,1)S(1)}, bf16[256,768]{1,0:T(8,128)(2,1)S(1)}, u32[]{:S(2)}, u32[]{:S(2)}) collective-permute-start(bf16[256,768]{1,0:T(8,128)(2,1)S(1)} %slice.9), channel_id=1, source_target_pairs={{0,64},{64,128},{128,192},{192,256},{256,320},{320,384},{384,448},... | collective-permute-start | bytes 1179656 | tf_op jit(solution)/shard_map/ppermute | solution.py:21
  101.2 0.0 copy-done.14
  101.2 0.0 copy-done.13
  101.2 0.6 reshape.28.scale_ref
  101.8 0.6 reshape.29.rate_ref
  102.4 0.8 reshape.34.extra_ref
  103.2 0.6 pad_add_fusion.place_ref
  103.8 0.0 collective-permute-done.partner_ref
  103.8 1.1 collective-permute-done.3.far_low_ref
  105.0 3.0 %collective-permute-done.4.far_high_ref = bf16[256,768]{1,0:T(8,128)(2,1)S(1)} collective-permute-done((bf16[256,768]{1,0:T(8,128)(2,1)S(1)}, bf16[256,768]{1,0:T(8,128)(2,1)S(1)}, u32[]{:S(2)}, u32[]{:S(2)}) %collective-permute-start.4) | collective-permute-done | bytes 393248 | tf_op jit(solution)/shard_map/ppermute | solution.py:21
  108.0 0.8 copy-done.7
  108.7 8.0 %shard_map.181 = (bf16[4,384,256]{2,1,0:T(8,128)(2,1)}, bf16[4,384,256]{2,1,0:T(8,128)(2,1)}) custom-call(s32[5]{0:T(128)} %pad_add_fusion.place_ref, bf16[4,384,256]{2,1,0:T(8,128)(2,1)} %copy-done.1, bf16[4,384,256]{2,1,0:T(8,128)(2,1)} %collective-permute-done.partner_ref, f32[4,2,1,256]{3,2,1,0:T(1,128)} %bitcast.12, bf16[512,768]{1,0:T(8,128)(2,1)} %bitcast.11, ...), custom_call_target="tpu_custom_call" | custom-call | flops 1207959552 | tf_op jit(solution)/shard_map/pallas_call | solution.py:226
  116.7 8.4 %collective-permute-start.5 = (bf16[4,384,256]{2,1,0:T(8,128)(2,1)}, bf16[4,384,256]{2,1,0:T(8,128)(2,1)S(1)}, u32[]{:S(2)}, u32[]{:S(2)}) collective-permute-start(bf16[4,384,256]{2,1,0:T(8,128)(2,1)} %get-tuple-element.10), channel_id=1, source_target_pairs={{0,1},{1,0},{2,3},{3,2},{4,5},{5,4},{6,7},{7,6},{8,9},{9,8},{10,11... | collective-permute-start | bytes 2359304 | tf_op jit(solution)/shard_map/ppermute | solution.py:33
  125.2 2.1 %collective-permute-done.5 = bf16[4,384,256]{2,1,0:T(8,128)(2,1)S(1)} collective-permute-done((bf16[4,384,256]{2,1,0:T(8,128)(2,1)}, bf16[4,384,256]{2,1,0:T(8,128)(2,1)S(1)}, u32[]{:S(2)}, u32[]{:S(2)}) %collective-permute-start.5) | collective-permute-done | bytes 786464 | tf_op jit(solution)/shard_map/ppermute | solution.py:33
  127.3 1.3 add_convert_fusion.1
  128.6 15.5 %all_to_all.26 = bf16[4,384,256]{2,1,0:T(8,128)(2,1)S(1)} all-to-all(bf16[4,384,256]{2,1,0:T(8,128)(2,1)S(1)} %add_convert_fusion.1), channel_id=1, replica_groups=mesh['rep'=2,'z'=4,'y'=8,'x'=4,'c'=2] {'x'}, dimensions={0} | all-to-all | bytes 1572864 | tf_op jit(solution)/shard_map/all_to_all | solution.py:25
  144.1 0.1 convert_reduce_fusion.1
  144.2 0.0 copy-start.10
  144.2 0.0 copy-start.11
  144.3 0.1 broadcast_in_dim.17
  144.3 13.0 %all_to_all.27.rows_ref = bf16[4,384,256]{2,1,0:T(8,128)(2,1)S(1)} all-to-all(bf16[4,384,256]{2,1,0:T(8,128)(2,1)S(1)} %broadcast_in_dim.17), channel_id=1, replica_groups=mesh['rep'=2,'z'=4,'y'=8,'x'=4,'c'=2] {'x'}, dimensions={0} | all-to-all | bytes 1572864 | tf_op jit(solution)/shard_map/all_to_all | solution.py:25
  157.3 4.6 %collective-permute-start.6 = (bf16[4,384,256]{2,1,0:T(8,128)(2,1)S(1)}, bf16[4,384,256]{2,1,0:T(8,128)(2,1)S(1)}, u32[]{:S(2)}, u32[]{:S(2)}) collective-permute-start(bf16[4,384,256]{2,1,0:T(8,128)(2,1)S(1)} %all_to_all.27.rows_ref), channel_id=1, source_target_pairs={{0,1},{1,0},{2,3},{3,2},{4,5},{5,4},{6,7},{7,6},{8,9},{9,8},{10,11... | collective-permute-start | bytes 2359304 | tf_op jit(solution)/shard_map/ppermute | solution.py:33
  161.9 0.6 reshape.32.gate_scale_ref
  162.5 0.6 reshape.33.up_scale_ref
  163.0 0.7 collective-permute-done.6.partner_ref
  163.8 0.9 copy-done.16
  164.7 9.7 %shard_map.182 = (bf16[4,384,256]{2,1,0:T(8,128)(2,1)}, bf16[4,384,256]{2,1,0:T(8,128)(2,1)}) custom-call(s32[5]{0:T(128)} %pad_add_fusion.place_ref, bf16[4,384,256]{2,1,0:T(8,128)(2,1)} %copy-done.5, bf16[4,384,256]{2,1,0:T(8,128)(2,1)} %copy-done.16, f32[4,2,1,256]{3,2,1,0:T(1,128)} %bitcast.13, ...), custom_call_target="tpu_custom_call" | custom-call | flops 3019898880 | tf_op jit(solution)/shard_map/pallas_call | solution.py:226
  174.4 2.3 %collective-permute-start.10 = (bf16[4,384,256]{2,1,0:T(8,128)(2,1)}, bf16[4,384,256]{2,1,0:T(8,128)(2,1)S(1)}, u32[]{:S(2)}, u32[]{:S(2)}) collective-permute-start(bf16[4,384,256]{2,1,0:T(8,128)(2,1)} %get-tuple-element.12), channel_id=1, source_target_pairs={{0,1},{1,0},{2,3},{3,2},{4,5},{5,4},{6,7},{7,6},{8,9},{9,8},{10,11... | collective-permute-start | bytes 2359304 | tf_op jit(solution)/shard_map/ppermute | solution.py:33
  176.7 2.1 %collective-permute-done.10 = bf16[4,384,256]{2,1,0:T(8,128)(2,1)S(1)} collective-permute-done((bf16[4,384,256]{2,1,0:T(8,128)(2,1)}, bf16[4,384,256]{2,1,0:T(8,128)(2,1)S(1)}, u32[]{:S(2)}, u32[]{:S(2)}) %collective-permute-start.10) | collective-permute-done | bytes 786464 | tf_op jit(solution)/shard_map/ppermute | solution.py:33
  178.8 1.3 add_convert_fusion
  180.1 14.4 %all_to_all.28 = bf16[4,384,256]{2,1,0:T(8,128)(2,1)S(1)} all-to-all(bf16[4,384,256]{2,1,0:T(8,128)(2,1)S(1)} %add_convert_fusion), channel_id=1, replica_groups=mesh['rep'=2,'z'=4,'y'=8,'x'=4,'c'=2] {'x'}, dimensions={0} | all-to-all | bytes 1572864 | tf_op jit(solution)/shard_map/all_to_all | solution.py:25
  194.5 0.1 convert_reduce_fusion
  194.6 0.7 add_convert_fusion.2
  (34 shorter events, 0.3 us)
Async XLA Ops:
  6.5 157.2 %all-gather.2.cloned.1.call-start = ((), (), s32[]{:S(2)}) async-start(), calls=%async_computation.5 | async-start | bytes 8847360 | tf_op jit(solution)/shard_map/all_gather | solution.py:59
  8.4 31.5 %copy-start.8 = (f32[64,384]{1,0:T(8,128)S(1)}, f32[64,384]{1,0:T(8,128)}, u32[]{:S(2)}) copy-start(f32[64,384]{1,0:T(8,128)} %param.21) | copy-start | bytes 294916
  9.5 30.4 %copy-start.9 = (f32[384,64]{0,1:T(8,128)S(1)}, f32[384,64]{0,1:T(8,128)}, u32[]{:S(2)}) copy-start(f32[384,64]{0,1:T(8,128)} %param.28) | copy-start | bytes 294916
  9.5 30.4 %copy-start.15 = (f32[64]{0:T(128)S(1)}, f32[64]{0:T(128)}, u32[]{:S(2)}) copy-start(f32[64]{0:T(128)} %param.29) | copy-start | bytes 772
  9.5 17.1 %collective-permute-start.7 = (bf16[64,1920]{1,0:T(8,128)(2,1)S(1)}, bf16[64,1920]{1,0:T(8,128)(2,1)S(1)}, u32[]{:S(2)}, u32[]{:S(2)}) collective-permute-start(bf16[64,1920]{1,0:T(8,128)(2,1)S(1)} %pad_maximum_fusion), channel_id=1, source_target_pairs={{0,64},{64,128},{128,192},{192,256},{256,320},{320,384},{384,448},... | collective-permute-start | bytes 737288 | tf_op jit(solution)/shard_map/ppermute | solution.py:21
  14.4 13.2 %collective-permute-start.8 = (bf16[64,1920]{1,0:T(8,128)(2,1)S(1)}, bf16[64,1920]{1,0:T(8,128)(2,1)S(1)}, u32[]{:S(2)}, u32[]{:S(2)}) collective-permute-start(bf16[64,1920]{1,0:T(8,128)(2,1)S(1)} %pad_maximum_fusion), channel_id=1, source_target_pairs={{0,448},{64,0},{128,64},{192,128},{256,192},{320,256},{384,320},{4... | collective-permute-start | bytes 737288 | tf_op jit(solution)/shard_map/ppermute | solution.py:21
  22.9 15.9 %collective-permute-start.9 = (bf16[64,1920]{1,0:T(8,128)(2,1)S(1)}, bf16[64,1920]{1,0:T(8,128)(2,1)S(1)}, u32[]{:S(2)}, u32[]{:S(2)}) collective-permute-start(bf16[64,1920]{1,0:T(8,128)(2,1)S(1)} %pad_maximum_fusion), channel_id=1, source_target_pairs={{0,128},{64,192},{128,256},{192,320},{256,384},{320,448},{384,0},{... | collective-permute-start | bytes 737288 | tf_op jit(solution)/shard_map/ppermute | solution.py:21
  38.8 1.0 copy-start.4
  39.9 32.3 %copy-start.6 = (bf16[384,256]{1,0:T(8,128)(2,1)S(1)}, bf16[384,256]{1,0:T(8,128)(2,1)}, u32[]{:S(2)}) copy-start(bf16[384,256]{1,0:T(8,128)(2,1)} %param.19) | copy-start | bytes 589828
  72.2 23.6 %copy-start = (bf16[8,64,768]{2,1,0:T(8,128)(2,1)}, bf16[8,64,768]{2,1,0:T(8,128)(2,1)S(1)}, u32[]{:S(2)}) copy-start(bf16[8,64,768]{2,1,0:T(8,128)(2,1)S(1)} %all_to_all.25) | copy-start | bytes 2359300
  73.2 28.0 %copy-start.14 = (f32[384]{0:T(512)S(1)}, f32[384]{0:T(512)}, u32[]{:S(2)}) copy-start(f32[384]{0:T(512)} %param.26) | copy-start | bytes 4612
  73.2 28.0 %copy-start.13 = (f32[384]{0:T(512)S(1)}, f32[384]{0:T(512)}, u32[]{:S(2)}) copy-start(f32[384]{0:T(512)} %param.22) | copy-start | bytes 4612
  73.2 29.2 %copy-start.12 = (f32[384]{0:T(512)S(1)}, f32[384]{0:T(512)}, u32[]{:S(2)}) copy-start(f32[384]{0:T(512)} %param.27) | copy-start | bytes 4612
  73.2 30.0 %copy-start.17 = (s32[4]{0:T(128)S(1)}, s32[4]{0:T(128)}, u32[]{:S(2)}) copy-start(s32[4]{0:T(128)} %constant.33.clone) | copy-start | bytes 52
  73.2 12.6 %all-to-all-start = ((bf16[4,384,256]{2,1,0:T(8,128)(2,1)}), bf16[4,384,256]{2,1,0:T(8,128)(2,1)S(1)}, u32[]{:S(2)}, u32[]{:S(2)}) async-start(bf16[4,384,256]{2,1,0:T(8,128)(2,1)} %broadcast_in_dim.15), calls=%async_computation | async-start | bytes 1572864 | tf_op jit(solution)/shard_map/all_to_all | solution.py:25
  77.4 17.5 %collective-permute-start.2 = (bf16[512,768]{1,0:T(8,128)(2,1)S(1)}, bf16[512,768]{1,0:T(8,128)(2,1)S(1)}, u32[]{:S(2)}, u32[]{:S(2)}) collective-permute-start(bf16[512,768]{1,0:T(8,128)(2,1)S(1)} %bitcast.9), channel_id=1, source_target_pairs={{0,448},{64,0},{128,64},{192,128},{256,192},{320,256},{384,320},{4... | collective-permute-start | bytes 2359304 | tf_op jit(solution)/shard_map/ppermute | solution.py:21
  79.3 18.4 %collective-permute-start.1 = (bf16[512,768]{1,0:T(8,128)(2,1)S(1)}, bf16[512,768]{1,0:T(8,128)(2,1)S(1)}, u32[]{:S(2)}, u32[]{:S(2)}) collective-permute-start(bf16[512,768]{1,0:T(8,128)(2,1)S(1)} %bitcast.10), channel_id=1, source_target_pairs={{0,64},{64,128},{128,192},{192,256},{256,320},{320,384},{384,448},... | collective-permute-start | bytes 2359304 | tf_op jit(solution)/shard_map/ppermute | solution.py:21
  85.8 22.1 %copy-start.1 = (bf16[4,384,256]{2,1,0:T(8,128)(2,1)}, bf16[4,384,256]{2,1,0:T(8,128)(2,1)S(1)}, u32[]{:S(2)}) copy-start(bf16[4,384,256]{2,1,0:T(8,128)(2,1)S(1)} %all-to-all-done.rows_ref) | copy-start | bytes 2359300
  85.8 18.0 %collective-permute-start = (bf16[4,384,256]{2,1,0:T(8,128)(2,1)S(1)}, bf16[4,384,256]{2,1,0:T(8,128)(2,1)}, u32[]{:S(2)}, u32[]{:S(2)}) collective-permute-start(bf16[4,384,256]{2,1,0:T(8,128)(2,1)S(1)} %all-to-all-done.rows_ref), channel_id=1, source_target_pairs={{0,1},{1,0},{2,3},{3,2},{4,5},{5,4},{6,7},{7,6},{8,9},{9,8},{10,11... | collective-permute-start | bytes 2359304 | tf_op jit(solution)/shard_map/ppermute | solution.py:33
  95.0 13.0 %copy-start.2 = (bf16[512,768]{1,0:T(8,128)(2,1)}, bf16[512,768]{1,0:T(8,128)(2,1)S(1)}, u32[]{:S(2)}) copy-start(bf16[512,768]{1,0:T(8,128)(2,1)S(1)} %collective-permute-done.2.after_ref) | copy-start | bytes 2359300
  95.8 9.1 %collective-permute-start.3 = (bf16[256,768]{1,0:T(8,128)(2,1)}, bf16[256,768]{1,0:T(8,128)(2,1)}, u32[]{:S(2)}, u32[]{:S(2)}) collective-permute-start(bf16[256,768]{1,0:T(8,128)(2,1)} %slice.8), channel_id=1, source_target_pairs={{0,448},{64,0},{128,64},{192,128},{256,192},{320,256},{384,320},{4... | collective-permute-start | bytes 1179656 | tf_op jit(solution)/shard_map/ppermute | solution.py:21
  97.8 10.2 %copy-start.3 = (bf16[512,768]{1,0:T(8,128)(2,1)}, bf16[512,768]{1,0:T(8,128)(2,1)S(1)}, u32[]{:S(2)}) copy-start(bf16[512,768]{1,0:T(8,128)(2,1)S(1)} %collective-permute-done.1.before_ref) | copy-start | bytes 2359300
  97.8 10.1 %collective-permute-start.4 = (bf16[256,768]{1,0:T(8,128)(2,1)S(1)}, bf16[256,768]{1,0:T(8,128)(2,1)S(1)}, u32[]{:S(2)}, u32[]{:S(2)}) collective-permute-start(bf16[256,768]{1,0:T(8,128)(2,1)S(1)} %slice.9), channel_id=1, source_target_pairs={{0,64},{64,128},{128,192},{192,256},{256,320},{320,384},{384,448},... | collective-permute-start | bytes 1179656 | tf_op jit(solution)/shard_map/ppermute | solution.py:21
  107.9 0.8 copy-start.7
  116.7 10.5 %collective-permute-start.5 = (bf16[4,384,256]{2,1,0:T(8,128)(2,1)}, bf16[4,384,256]{2,1,0:T(8,128)(2,1)S(1)}, u32[]{:S(2)}, u32[]{:S(2)}) collective-permute-start(bf16[4,384,256]{2,1,0:T(8,128)(2,1)} %get-tuple-element.10), channel_id=1, source_target_pairs={{0,1},{1,0},{2,3},{3,2},{4,5},{5,4},{6,7},{7,6},{8,9},{9,8},{10,11... | collective-permute-start | bytes 2359304 | tf_op jit(solution)/shard_map/ppermute | solution.py:33
  144.2 17.7 %copy-start.10 = (f32[640]{0:T(1024)S(1)}, f32[640]{0:T(1024)}, u32[]{:S(2)}) copy-start(f32[640]{0:T(1024)} %param.32) | copy-start | bytes 7684
  144.2 18.3 %copy-start.11 = (f32[640]{0:T(1024)S(1)}, f32[640]{0:T(1024)}, u32[]{:S(2)}) copy-start(f32[640]{0:T(1024)} %param.34) | copy-start | bytes 7684
  157.3 6.5 %copy-start.5 = (bf16[4,384,256]{2,1,0:T(8,128)(2,1)}, bf16[4,384,256]{2,1,0:T(8,128)(2,1)S(1)}, u32[]{:S(2)}) copy-start(bf16[4,384,256]{2,1,0:T(8,128)(2,1)S(1)} %all_to_all.27.rows_ref) | copy-start | bytes 2359300
  157.3 6.5 %collective-permute-start.6 = (bf16[4,384,256]{2,1,0:T(8,128)(2,1)S(1)}, bf16[4,384,256]{2,1,0:T(8,128)(2,1)S(1)}, u32[]{:S(2)}, u32[]{:S(2)}) collective-permute-start(bf16[4,384,256]{2,1,0:T(8,128)(2,1)S(1)} %all_to_all.27.rows_ref), channel_id=1, source_target_pairs={{0,1},{1,0},{2,3},{3,2},{4,5},{5,4},{6,7},{7,6},{8,9},{9,8},{10,11... | collective-permute-start | bytes 2359304 | tf_op jit(solution)/shard_map/ppermute | solution.py:33
  163.8 0.9 copy-start.16
  174.4 4.4 %collective-permute-start.10 = (bf16[4,384,256]{2,1,0:T(8,128)(2,1)}, bf16[4,384,256]{2,1,0:T(8,128)(2,1)S(1)}, u32[]{:S(2)}, u32[]{:S(2)}) collective-permute-start(bf16[4,384,256]{2,1,0:T(8,128)(2,1)} %get-tuple-element.12), channel_id=1, source_target_pairs={{0,1},{1,0},{2,3},{3,2},{4,5},{5,4},{6,7},{7,6},{8,9},{9,8},{10,11... | collective-permute-start | bytes 2359304 | tf_op jit(solution)/shard_map/ppermute | solution.py:33
Sparse Core Ops, SparseCore 0:
  40.0 101.8 all-gather.1
where the time goes:
time: 203 us; the launch traced here: 202 us
  blocking collectives  75 us (37%)
  starting transfers between devices  54.5 us (27%)
  waiting for transfers between devices  26 us (13%)
  Pallas kernels  17.7 us (9%)
  between operations  13.7 us (7%)
  local copies, waits for them, and re-layouts  7.95 us (4%)
  other arithmetic  7.28 us (4%)
    all_to_all x4, blocking collectives, swap(): return lax.all_to_all(value, axis, split_axis=0, concat_axis=0, tiled=True)  75 us
    ppermute x7, starting transfers between devices, shift_z(): lax.ppermute(value, ('rep', 'z'), [(i, (i + step) % count) for i in range...  25.9 us
    ppermute x4, starting transfers between devices, to_partner(): return lax.ppermute(value, 'c', [(0, 1), (1, 0)])  24.4 us
    ppermute x7, waiting for transfers between devices, shift_z(): lax.ppermute(value, ('rep', 'z'), [(i, (i + step) % count) for i in range...  18 us
    pallas_call x2, Pallas kernels, call(): pl.pallas_call(kernel, out_shape=[jax.ShapeDtypeStruct((4, rows, width),...  17.7 us
    ppermute x4, waiting for transfers between devices, to_partner(): return lax.ppermute(value, 'c', [(0, 1), (1, 0)])  4.91 us
    all_to_all x1, starting transfers between devices, swap(): return lax.all_to_all(value, axis, split_axis=0, concat_axis=0, tiled=True)  4.19 us
  transfers between devices with their start and end apart: 13, of which 9 were waited for; matrix products, arithmetic and copies ran while one was open for 4% of the time, Pallas kernels for 4%

commit v1 on v0

v1 whole, which is shorter than its diff:
```python
import jax
import jax.numpy as jnp
from jax import lax
from jax.experimental import pallas as pl
from jax.experimental.pallas import tpu as pltpu
from jax.sharding import Mesh
from jax.sharding import PartitionSpec as P

FS = ("z", "y")
TP = ("x", "c")
REP_FS = ("rep", "z", "y")
EPS = 1e-06
DECAY_FACTOR = 8.0
CHUNKS = 8
PIECES = 4
F32 = jnp.float32
BF16 = jnp.bfloat16


def shift_z(value, step):
    count = lax.axis_size("rep") * lax.axis_size("z")
    return lax.ppermute(value, ("rep", "z"), [(i, (i + step) % count) for i in range(count)])


def swap(value, axis):
    return lax.all_to_all(value, axis, split_axis=0, concat_axis=0, tiled=True)


def copies_to(value, axis):
    return swap(jnp.broadcast_to(value, (lax.axis_size(axis), *value.shape)), axis)


def to_partner(value):
    return lax.ppermute(value, "c", [(0, 1), (1, 0)])


def chips_in_order(block):
    return copies_to(block, "x")


def shift_x(value, step):
    count = lax.axis_size("x")
    return lax.ppermute(value, "x", [(i, (i + step) % count) for i in range(count)])


def chips_from_here(block):
    far = shift_x(block, 2)
    near = (block, shift_x(block, 1), shift_x(block, -1), far)
    return jnp.stack(near)


def share_sums(kept, sent):
    pair = (kept.astype(F32) + to_partner(sent).astype(F32)).astype(BF16)
    return swap(pair, "x").astype(F32).sum(axis=0)


def over_z(own, step):
    before = shift_z(own, 1)
    after = shift_z(own, -1)
    far = shift_z(before if step > 0 else after, step)
    return own, before, after, far


def over_plane(mine, other):
    piece = jnp.where(lax.axis_index("rep") == 0, mine, other).astype(BF16)
    return lax.all_gather(piece, ("rep", *FS), axis=0, tiled=True)


def dot(a, b):
    return jnp.dot(a, b, preferred_element_type=F32)


def dot_t(a, b):
    return lax.dot_general(a, b, (((1,), (1,)), ((), ())), preferred_element_type=F32)


def normalize(blocks, gain_ref, normed_ref):
    width = blocks[0][0].shape[1]
    total = None
    for block, _, _ in blocks:
        v = block[...].astype(F32)
        square = v * v
        for start in range(0, width, 128):
            part = square[:, start : start + 128]
            total = part if total is None else total + part
    mean = jnp.sum(total, axis=-1, keepdims=True) / (len(blocks) * width)
    inverse = lax.rsqrt(mean + EPS)
    for block, x, c in blocks:
        v = block[...].astype(F32)
        normed_ref[x, c] = (v * inverse * gain_ref[x, c]).astype(BF16)


def halves(normed_ref, chip):
    return jnp.concatenate([normed_ref[chip, 0], normed_ref[chip, 1]], axis=1)


def nearby(axis):
    here = lax.axis_index(axis)
    return [lax.rem(here + step, 4) for step in (0, 3, 1, 2)]


def recurrence_kernel(
    rows_ref,
    partner_ref,
    gain_ref,
    own_ref,
    before_ref,
    after_ref,
    far_ref,
    scale_ref,
    taps_ref,
    recur_ref,
    input_ref,
    rate_ref,
    extra_ref,
    state_ref,
    normed_ref,
    padded_ref,
    decay_ref,
    value_ref,
):
    rows = rows_ref.shape[1]
    width = own_ref.shape[1]
    core = lax.axis_index("c")
    chips = nearby("x")
    blocks = [(rows_ref.at[i], chip, core) for i, chip in enumerate(chips)]
    blocks += [(partner_ref.at[i], chip, 1 - core) for i, chip in enumerate(chips)]
    normalize(blocks, gain_ref, normed_ref)
    total = None
    for place, ref in zip(nearby("z"), (own_ref, before_ref, after_ref, far_ref)):
        part = dot(halves(normed_ref, place), ref[...])
        total = part if total is None else total + part
    taps = taps_ref.shape[0]
    padded_ref[0:8, :] = jnp.zeros((8, width), F32)
    padded_ref[8:, :] = (total * lanes(scale_ref)).astype(BF16).astype(F32)
    conv = None
    for k in range(taps):
        start = 8 - (taps - 1) + k
        term = taps_ref[k : k + 1, :] * padded_ref[start : start + rows, :]
        conv = term if conv is None else conv + term
    low = conv.astype(BF16)
    size = recur_ref.shape[1]
    extra = [
        jnp.broadcast_to(extra_ref[i], (size, size)).T for i in range(extra_ref.shape[0])
    ]
    extra = jnp.concatenate(extra, axis=0)
    for n in range(recur_ref.shape[0]):
        cols = slice(n * size, (n + 1) * size)
        gate = jax.nn.sigmoid(dot(low[:, cols], recur_ref[n]))
        chosen = jax.nn.sigmoid(dot(low[:, cols], input_ref[n]))
        logarithm = gate * rate_ref[n] + extra
        decay = jnp.exp(logarithm)
        rest = jnp.tanh(-logarithm) * (1.0 + decay * decay)
        decay_ref[n] = decay
        value_ref[n] = jnp.sqrt(rest) * chosen * conv[:, cols]
    count = recur_ref.shape[0]
    steps = rows // CHUNKS

    def step(t, carry):
        new = []
        for n in range(count):
            at = (n, pl.ds(t, CHUNKS, stride=steps), slice(None))
            decay = decay_ref[at]
            state = decay * carry[2 * n] + value_ref[at]
            product = decay * carry[2 * n + 1]
            value_ref[at] = state
            decay_ref[at] = product
            new += [state, product]
        return tuple(new)

    first = (jnp.zeros((CHUNKS, size), F32), jnp.ones((CHUNKS, size), F32)) * count
    ends = lax.fori_loop(0, steps, step, first, unroll=8)
    for n in range(count):
        state, product = ends[2 * n], ends[2 * n + 1]
        cols = slice(n * size, (n + 1) * size)
        enter = jnp.zeros((1, size), F32)
        for chunk in range(CHUNKS):
            span = slice(chunk * steps, (chunk + 1) * steps)
            whole = value_ref[n, span, :] + decay_ref[n, span, :] * enter
            state_ref[span, cols] = whole.astype(BF16)
            enter = state[chunk : chunk + 1] + product[chunk : chunk + 1] * enter


def mixing_kernel(
    state_ref,
    own_ref,
    before_ref,
    after_ref,
    far_ref,
    kept_hbm,
    sent_hbm,
    kept_ref,
    sent_ref,
    sems,
):
    out = Parts(kept_hbm, sent_hbm, kept_ref, sent_ref, sems)
    low = state_ref[...]
    for place, ref in zip(nearby("z"), (own_ref, before_ref, after_ref, far_ref)):
        out.put(place, lambda span: dot_t(low, ref[span, :]))
    out.wait()


def ffn_kernel(
    rows_ref,
    partner_ref,
    gain_ref,
    gate_scale_ref,
    up_scale_ref,
    weights_hbm,
    kept_hbm,
    sent_hbm,
    kept_ref,
    sent_ref,
    out_sems,
    normed_ref,
    in_ref,
    out_ref,
    sems,
):
    width = in_ref.shape[2]
    deep = in_ref.shape[1]
    step = deep // PIECES
    copies = []
    for first, target in ((0, in_ref), (width, out_ref)):
        for side in range(2):
            for piece in range(PIECES):
                span = pl.ds(side * deep + piece * step, step)
                source = weights_hbm.at[span, pl.ds(first, target.shape[2])]
                kept = target.at[side, pl.ds(piece * step, step)]
                copy = pltpu.make_async_copy(source, kept, sems.at[len(copies)])
                copy.start()
                copies.append(copy)

    def arrived(group):
        for copy in copies[group * PIECES : (group + 1) * PIECES]:
            copy.wait()

    core = lax.axis_index("c")
    chips = rows_ref.shape[0]
    blocks = [(rows_ref.at[i], i, core) for i in range(chips)]
    blocks += [(partner_ref.at[i], i, 1 - core) for i in range(chips)]
    normalize(blocks, gain_ref, normed_ref)
    left = jnp.concatenate([halves(normed_ref, x) for x in range(chips)], axis=1)
    arrived(0)
    gate = dot(left, in_ref[0]) * lanes(gate_scale_ref)
    arrived(1)
    up = dot(left, in_ref[1]) * lanes(up_scale_ref)
    hidden = (gate * jax.nn.sigmoid(gate) * up).astype(BF16)
    first, second = hidden[:, : width // 2], hidden[:, width // 2 :]
    arrived(2)
    arrived(3)
    span = deep // chips
    out = Parts(kept_hbm, sent_hbm, kept_ref, sent_ref, out_sems)
    for x in range(chips):

        def product(rows):
            one = dot_t(first, out_ref[0, rows])
            return one + dot_t(second, out_ref[1, rows])

        out.put(x, product, x * span)
    out.wait()


def lanes(ref):
    return jnp.concatenate([ref[n] for n in range(ref.shape[0])], axis=1)


class Parts:
    def __init__(self, kept_hbm, sent_hbm, kept_ref, sent_ref, sems):
        core = lax.axis_index("c")
        self.sides = ((core, kept_ref, kept_hbm), (1 - core, sent_ref, sent_hbm))
        self.width = kept_ref.shape[2]
        self.sems = sems
        self.copies = []

    def put(self, place, product, base=0):
        for half, ref, out in self.sides:
            start = pl.multiple_of(base + half * self.width, self.width)
            ref[place] = product(pl.ds(start, self.width)).astype(BF16)
            sem = self.sems.at[len(self.copies)]
            copy = pltpu.make_async_copy(ref.at[place], out.at[place], sem)
            copy.start()
            self.copies.append(copy)

    def wait(self):
        for copy in self.copies:
            copy.wait()


def call(kernel, small, large, outs, scratch, flops):
    vmem = pl.BlockSpec(memory_space=pltpu.VMEM)
    hbm = pl.BlockSpec(memory_space=pl.ANY)
    out_specs = [vmem]
    if len(outs) > 1:
        out_specs = [hbm] * len(outs)
        scratch = [pltpu.VMEM(shape, BF16) for shape in outs] + [
            pltpu.SemaphoreType.DMA((8,)),
            *scratch,
        ]
    return pl.pallas_call(
        kernel,
        out_shape=[jax.ShapeDtypeStruct(shape, BF16) for shape in outs],
        in_specs=[vmem] * len(small) + [hbm] * len(large),
        out_specs=out_specs,
        scratch_shapes=scratch,
        compiler_params=pltpu.CompilerParams(vmem_limit_bytes=56 * 1024 * 1024),
        cost_estimate=pl.CostEstimate(flops=flops, transcendentals=0, bytes_accessed=0),
    )(*small, *large)


def layer(
    tokens,
    mixing_norm_gain,
    recurrent_input_weight,
    recurrent_input_scale,
    convolution_kernel_taps,
    recurrence_gate_weight_blocks,
    input_gate_weight_blocks,
    channel_decay_parameter,
    token_extra_log_decay,
    mixing_output_weight,
    mixing_output_scale,
    feedforward_norm_gain,
    feedforward_gate_weight,
    feedforward_gate_scale,
    feedforward_up_weight,
    feedforward_up_scale,
    feedforward_down_weight,
    feedforward_down_scale,
):
    rows, features = tokens.shape
    width = recurrent_input_weight.shape[1]
    mix_rows = (mixing_output_weight * mixing_output_scale).T
    pair = jnp.stack([recurrent_input_weight, mix_rows]).astype(BF16)
    down = (feedforward_down_weight * feedforward_down_scale).T
    half = down.shape[1] // 2
    ffn_blocks = over_plane(
        jnp.concatenate([feedforward_gate_weight, down[:, :half]], axis=1),
        jnp.concatenate([feedforward_up_weight, down[:, half:]], axis=1),
    )

    pair = copies_to(pair, "y")
    rec_blocks = over_z(pair[:, 0].reshape(-1, width), 1)
    mix_blocks = over_z(pair[:, 1].reshape(-1, width), -1)
    rate = -DECAY_FACTOR * jax.nn.softplus(-channel_decay_parameter)
    count, size = recurrence_gate_weight_blocks.shape[:2]
    tok = chips_from_here(tokens)
    terms = [(4, rows, features)] * 2
    normed = pltpu.VMEM((4, 2, rows, features), BF16)
    (state,) = call(
        recurrence_kernel,
        (
            tok,
            to_partner(tok),
            mixing_norm_gain.reshape(4, 2, 1, -1),
            *rec_blocks,
            recurrent_input_scale.reshape(-1, 1, size),
            convolution_kernel_taps,
            recurrence_gate_weight_blocks,
            input_gate_weight_blocks,
            rate.reshape(-1, 1, size),
            token_extra_log_decay.reshape(-1, 1, size),
        ),
        (),
        [(rows, width)],
        [
            normed,
            pltpu.VMEM((rows + 8, width), F32),
            pltpu.VMEM((count, rows, size), F32),
            pltpu.VMEM((count, rows, size), F32),
        ],
        2 * rows * width * features * 8,
    )
    mix_terms = call(
        mixing_kernel,
        (state, *mix_blocks),
        (),
        terms,
        [],
        2 * rows * width * features * 8,
    )
    mixed = (tokens.astype(F32) + share_sums(*mix_terms)).astype(BF16)
    mid = chips_in_order(mixed)
    hidden_width = feedforward_gate_weight.shape[1]
    down_terms = call(
        ffn_kernel,
        (
            mid,
            to_partner(mid),
            feedforward_norm_gain.reshape(4, 2, 1, -1),
            feedforward_gate_scale.reshape(-1, 1, size),
            feedforward_up_scale.reshape(-1, 1, size),
        ),
        (ffn_blocks,),
        terms,
        [
            normed,
            pltpu.VMEM((2, 8 * features, hidden_width), BF16),
            pltpu.VMEM((2, 8 * features, hidden_width // 2), BF16),
            pltpu.SemaphoreType.DMA((4 * PIECES,)),
        ],
        6 * rows * hidden_width * features * 8,
    )
    return (mixed.astype(F32) + share_sums(*down_terms)).astype(BF16)


def solution(mesh):
    torus = Mesh(
        mesh.devices.reshape(mesh.shape["rep"], 4, 8, 4, 2), ("rep", "z", "y", "x", "c")
    )
    return jax.shard_map(
        layer,
        mesh=torus,
        in_specs=(
            P(REP_FS, TP),
            P(),
            P(FS, TP),
            P(TP),
            P(None, TP),
            P(TP, None, None),
            P(TP, None, None),
            P(TP),
            P(REP_FS),
            P(TP, FS),
            P(FS),
            P(),
            P(FS, TP),
            P(TP),
            P(FS, TP),
            P(TP),
            P(TP, FS),
            P(FS),
        ),
        out_specs=P(REP_FS, TP),
        check_vma=False,
    )
```

time: 203 us -> 186 us (0.916)
  blocking collectives: 75 us -> 42.8 us
  starting transfers between devices: 54.5 us -> 66.6 us
  waiting for transfers between devices: 26 us -> 28.1 us
    all_to_all x4 -> x3, blocking collectives: 75 us -> 42.8 us  [swap(): return lax.all_to_all(value, axis, split_axis=0, concat_axis=0, tiled=True)]
    ppermute x0 -> x3, starting transfers between devices: none -> 9.93 us  [shift_x(): lax.ppermute(value, 'x', [(i, (i + step) % count) for i in range(count)])]
    ppermute x0 -> x3, waiting for transfers between devices: none -> 4.75 us  [shift_x(): lax.ppermute(value, 'x', [(i, (i + step) % count) for i in range(count)])]
    ppermute x4, starting transfers between devices: 24.4 us -> 20.8 us  [to_partner(): return lax.ppermute(value, 'c', [(0, 1), (1, 0)])]
    all_to_all x1, starting transfers between devices: 4.19 us -> 7.64 us  [swap(): return lax.all_to_all(value, axis, split_axis=0, concat_axis=0, tiled=True)]
    unnamed x3 -> x0, other arithmetic: 2.92 us -> none
    ppermute x7 -> x6, starting transfers between devices: 25.9 us -> 28.2 us  [shift_z(): lax.ppermute(value, ('rep', 'z'), [(i, (i + step) % count) for i in range...]
    all_to_all x1, waiting for transfers between devices: 3.11 us -> 1.06 us  [swap(): return lax.all_to_all(value, axis, split_axis=0, concat_axis=0, tiled=True)]
  transfers between devices with their start and end apart: 13 -> 15, of which waited for: 9 -> 9; matrix products, arithmetic and copies ran while one was open for 4% -> 5% of each run, Pallas kernels for 4% -> 5%
where the time goes in v1:
time: 186 us; the launch traced here: 185 us
  starting transfers between devices  66.6 us (36%)
  blocking collectives  42.8 us (23%)
  waiting for transfers between devices  28.1 us (15%)
  Pallas kernels  18.7 us (10%)
  between operations  13.7 us (7%)
  other arithmetic  8.34 us (4%)
  local copies, waits for them, and re-layouts  6.7 us (4%)
    all_to_all x3, blocking collectives, swap(): return lax.all_to_all(value, axis, split_axis=0, concat_axis=0, tiled=True)  42.8 us
    ppermute x6, starting transfers between devices, shift_z(): lax.ppermute(value, ('rep', 'z'), [(i, (i + step) % count) for i in range...  28.2 us
    ppermute x4, starting transfers between devices, to_partner(): return lax.ppermute(value, 'c', [(0, 1), (1, 0)])  20.8 us
    pallas_call x3, Pallas kernels, call(): pl.pallas_call(kernel, out_shape=[jax.ShapeDtypeStruct(shape, BF16) for s...  18.7 us
    ppermute x6, waiting for transfers between devices, shift_z(): lax.ppermute(value, ('rep', 'z'), [(i, (i + step) % count) for i in range...  17.4 us
    ppermute x3, starting transfers between devices, shift_x(): lax.ppermute(value, 'x', [(i, (i + step) % count) for i in range(count)])  9.93 us
    all_to_all x1, starting transfers between devices, swap(): return lax.all_to_all(value, axis, split_axis=0, concat_axis=0, tiled=True)  7.64 us
    ppermute x4, waiting for transfers between devices, to_partner(): return lax.ppermute(value, 'c', [(0, 1), (1, 0)])  4.9 us
  transfers between devices with their start and end apart: 15, of which 9 were waited for; matrix products, arithmetic and copies ran while one was open for 5% of the time, Pallas kernels for 5%

profile of v1, /device:TPU:1, one launch (start us, length us, event | category | flops | bytes accessed | tf_op | source)
XLA Modules:
  0.0 184.8 jit_solution(12910402277603287234)
XLA Ops:
  6.5 0.0 all-gather.2.cloned.1.call-start
  6.5 1.0 multiply_bitcast_fusion
  7.5 0.1 fusion.4
  7.6 1.7 fusion
  9.3 0.0 all-gather.2.cloned.1.call-update
  9.3 0.9 convert_bitcast_fusion
  10.3 1.0 fusion.1
  11.3 1.0 broadcast_in_dim.8
  12.3 7.6 %all-to-all-start = ((bf16[8,2,64,384]{3,2,1,0:T(8,128)(2,1)}), bf16[8,2,64,384]{3,2,1,0:T(8,128)(2,1)S(1)}, u32[]{:S(2)}, u32[]{:S(2)}) async-start(bf16[8,2,64,384]{3,2,1,0:T(8,128)(2,1)} %broadcast_in_dim.8), calls=%async_computation | async-start | bytes 1572864 | tf_op jit(solution)/shard_map/all_to_all | solution.py:26
  19.9 0.0 copy-done.4
  19.9 3.1 %collective-permute-start = (bf16[384,256]{1,0:T(8,128)(2,1)S(1)}, bf16[384,256]{1,0:T(8,128)(2,1)S(1)}, u32[]{:S(2)}, u32[]{:S(2)}) collective-permute-start(bf16[384,256]{1,0:T(8,128)(2,1)S(1)} %copy-done.4), channel_id=1, source_target_pairs={{0,2},{2,4},{4,6},{6,0},{1,3},{3,5},{5,7},{7,1},{8,10},{10,12},{12... | collective-permute-start | bytes 589832 | tf_op jit(solution)/shard_map/ppermute | solution.py:43
  23.1 3.4 %collective-permute-start.1 = (bf16[384,256]{1,0:T(8,128)(2,1)S(1)}, bf16[384,256]{1,0:T(8,128)(2,1)S(1)}, u32[]{:S(2)}, u32[]{:S(2)}) collective-permute-start(bf16[384,256]{1,0:T(8,128)(2,1)S(1)} %copy-done.4), channel_id=1, source_target_pairs={{0,6},{2,0},{4,2},{6,4},{1,7},{3,1},{5,3},{7,5},{8,14},{10,8},{12,... | collective-permute-start | bytes 589832 | tf_op jit(solution)/shard_map/ppermute | solution.py:43
  26.5 3.4 %collective-permute-start.2 = (bf16[384,256]{1,0:T(8,128)(2,1)S(1)}, bf16[384,256]{1,0:T(8,128)(2,1)S(1)}, u32[]{:S(2)}, u32[]{:S(2)}) collective-permute-start(bf16[384,256]{1,0:T(8,128)(2,1)S(1)} %copy-done.4), channel_id=1, source_target_pairs={{0,4},{2,6},{4,0},{6,2},{1,5},{3,7},{5,1},{7,3},{8,12},{10,14},{12... | collective-permute-start | bytes 589832 | tf_op jit(solution)/shard_map/ppermute | solution.py:43
  29.9 0.0 collective-permute-done
  29.9 0.0 collective-permute-done.1
  29.9 4.7 %collective-permute-done.2 = bf16[384,256]{1,0:T(8,128)(2,1)S(1)} collective-permute-done((bf16[384,256]{1,0:T(8,128)(2,1)S(1)}, bf16[384,256]{1,0:T(8,128)(2,1)S(1)}, u32[]{:S(2)}, u32[]{:S(2)}) %collective-permute-start.2) | collective-permute-done | bytes 196640 | tf_op jit(solution)/shard_map/ppermute | solution.py:43
  34.7 0.1 pad_maximum_fusion.rows_ref
  34.8 0.0 copy-start
  34.8 6.1 %collective-permute-start.3 = (bf16[4,384,256]{2,1,0:T(8,128)(2,1)S(1)}, bf16[4,384,256]{2,1,0:T(8,128)(2,1)S(1)}, u32[]{:S(2)}, u32[]{:S(2)}) collective-permute-start(bf16[4,384,256]{2,1,0:T(8,128)(2,1)S(1)} %pad_maximum_fusion.rows_ref), channel_id=1, source_target_pairs={{0,1},{1,0},{2,3},{3,2},{4,5},{5,4},{6,7},{7,6},{8,9},{9,8},{10,11... | collective-permute-start | bytes 2359304 | tf_op jit(solution)/shard_map/ppermute | solution.py:34
  40.9 1.1 all-to-all-done
  41.9 0.9 fusion.3
  42.8 7.2 %collective-permute-start.4 = (bf16[512,384]{1,0:T(8,128)(2,1)S(1)}, bf16[512,384]{1,0:T(8,128)(2,1)S(1)}, u32[]{:S(2)}, u32[]{:S(2)}) collective-permute-start(bf16[512,384]{1,0:T(8,128)(2,1)S(1)} %bitcast.16), channel_id=1, source_target_pairs={{0,64},{64,128},{128,192},{192,256},{256,320},{320,384},{384,448},... | collective-permute-start | bytes 1179656 | tf_op jit(solution)/shard_map/ppermute | solution.py:22
  50.0 9.2 %collective-permute-start.8 = (bf16[512,384]{1,0:T(8,128)(2,1)}, bf16[512,384]{1,0:T(8,128)(2,1)}, u32[]{:S(2)}, u32[]{:S(2)}) collective-permute-start(bf16[512,384]{1,0:T(8,128)(2,1)} %bitcast.9.own_ref), channel_id=1, source_target_pairs={{0,448},{64,0},{128,64},{192,128},{256,192},{320,256},{384,320},{4... | collective-permute-start | bytes 1179656 | tf_op jit(solution)/shard_map/ppermute | solution.py:22
  59.3 3.4 %collective-permute-start.5 = (bf16[512,384]{1,0:T(8,128)(2,1)S(1)}, bf16[512,384]{1,0:T(8,128)(2,1)S(1)}, u32[]{:S(2)}, u32[]{:S(2)}) collective-permute-start(bf16[512,384]{1,0:T(8,128)(2,1)S(1)} %bitcast.17), channel_id=1, source_target_pairs={{0,448},{64,0},{128,64},{192,128},{256,192},{320,256},{384,320},{4... | collective-permute-start | bytes 1179656 | tf_op jit(solution)/shard_map/ppermute | solution.py:22
  62.6 4.0 %collective-permute-done.4.before_ref = bf16[512,384]{1,0:T(8,128)(2,1)S(1)} collective-permute-done((bf16[512,384]{1,0:T(8,128)(2,1)S(1)}, bf16[512,384]{1,0:T(8,128)(2,1)S(1)}, u32[]{:S(2)}, u32[]{:S(2)}) %collective-permute-start.4) | collective-permute-done | bytes 393248 | tf_op jit(solution)/shard_map/ppermute | solution.py:22
  66.6 1.9 %collective-permute-start.6 = (bf16[512,384]{1,0:T(8,128)(2,1)S(1)}, bf16[512,384]{1,0:T(8,128)(2,1)S(1)}, u32[]{:S(2)}, u32[]{:S(2)}) collective-permute-start(bf16[512,384]{1,0:T(8,128)(2,1)S(1)} %collective-permute-done.4.before_ref), channel_id=1, source_target_pairs={{0,64},{64,128},{128,192},{192,256},{256,320},{320,384},{384,448},... | collective-permute-start | bytes 1179656 | tf_op jit(solution)/shard_map/ppermute | solution.py:22
  68.5 1.9 %collective-permute-start.7 = (bf16[512,384]{1,0:T(8,128)(2,1)}, bf16[512,384]{1,0:T(8,128)(2,1)}, u32[]{:S(2)}, u32[]{:S(2)}) collective-permute-start(bf16[512,384]{1,0:T(8,128)(2,1)} %bitcast.9.own_ref), channel_id=1, source_target_pairs={{0,64},{64,128},{128,192},{192,256},{256,320},{320,384},{384,448},... | collective-permute-start | bytes 1179656 | tf_op jit(solution)/shard_map/ppermute | solution.py:22
  70.5 0.0 collective-permute-done.8.after_ref
  70.5 4.6 %collective-permute-start.9 = (bf16[512,384]{1,0:T(8,128)(2,1)}, bf16[512,384]{1,0:T(8,128)(2,1)}, u32[]{:S(2)}, u32[]{:S(2)}) collective-permute-start(bf16[512,384]{1,0:T(8,128)(2,1)} %collective-permute-done.8.after_ref), channel_id=1, source_target_pairs={{0,448},{64,0},{128,64},{192,128},{256,192},{320,256},{384,320},{4... | collective-permute-start | bytes 1179656 | tf_op jit(solution)/shard_map/ppermute | solution.py:22
  75.0 0.0 copy-done.12
  75.1 0.6 reshape.25.rate_ref
  75.7 0.0 copy-done.10
  75.7 0.6 reshape.24.scale_ref
  76.3 0.0 copy-done.11
  76.3 0.6 reshape.26.extra_ref
  76.9 0.0 collective-permute-done.3.partner_ref
  76.9 0.6 collective-permute-done.5.after_ref
  77.5 2.7 %collective-permute-done.6.far_ref = bf16[512,384]{1,0:T(8,128)(2,1)S(1)} collective-permute-done((bf16[512,384]{1,0:T(8,128)(2,1)S(1)}, bf16[512,384]{1,0:T(8,128)(2,1)S(1)}, u32[]{:S(2)}, u32[]{:S(2)}) %collective-permute-start.6) | collective-permute-done | bytes 393248 | tf_op jit(solution)/shard_map/ppermute | solution.py:22
  80.2 0.7 copy-done.7
  81.0 6.0 %shard_map.172.state_ref = bf16[384,384]{1,0:T(8,128)(2,1)} custom-call(bf16[4,384,256]{2,1,0:T(8,128)(2,1)} %copy-done, bf16[4,384,256]{2,1,0:T(8,128)(2,1)} %copy-done.2, f32[4,2,1,256]{3,2,1,0:T(1,128)} %bitcast.23, bf16[512,384]{1,0:T(8,128)(2,1)} %bitcast.18, bf16[512,384]{1,0:T(8,128)(2,1)} %copy-done.5, bf16[512,384]{1,0:T(8,128)(2,1)} %copy-done.6, ...), custom_call_target="tpu_custom_call" | custom-call | flops 603979776 | tf_op jit(solution)/shard_map/pallas_call | solution.py:300
  86.9 10.1 %collective-permute-done.7.before_ref = bf16[512,384]{1,0:T(8,128)(2,1)} collective-permute-done((bf16[512,384]{1,0:T(8,128)(2,1)}, bf16[512,384]{1,0:T(8,128)(2,1)}, u32[]{:S(2)}, u32[]{:S(2)}) %collective-permute-start.7) | collective-permute-done | bytes 393248 | tf_op jit(solution)/shard_map/ppermute | solution.py:22
  97.0 0.0 collective-permute-done.9.far_ref
  97.0 3.3 %shard_map.173 = (bf16[4,384,256]{2,1,0:T(8,128)(2,1)}, bf16[4,384,256]{2,1,0:T(8,128)(2,1)}) custom-call(bf16[384,384]{1,0:T(8,128)(2,1)} %shard_map.172.state_ref, bf16[512,384]{1,0:T(8,128)(2,1)} %bitcast.9.own_ref, bf16[512,384]{1,0:T(8,128)(2,1)} %collective-permute-done.7.before_ref, bf16[512,384]{1,0:T(8,128)(2,1)} %collective-permute-done.8.after_ref, ...), custom_call_target="tpu_custom_call" | custom-call | flops 603979776 | tf_op jit(solution)/shard_map/pallas_call | solution.py:300
  100.3 7.9 %collective-permute-start.10 = (bf16[4,384,256]{2,1,0:T(8,128)(2,1)}, bf16[4,384,256]{2,1,0:T(8,128)(2,1)S(1)}, u32[]{:S(2)}, u32[]{:S(2)}) collective-permute-start(bf16[4,384,256]{2,1,0:T(8,128)(2,1)} %get-tuple-element.10), channel_id=1, source_target_pairs={{0,1},{1,0},{2,3},{3,2},{4,5},{5,4},{6,7},{7,6},{8,9},{9,8},{10,11... | collective-permute-start | bytes 2359304 | tf_op jit(solution)/shard_map/ppermute | solution.py:34
  108.3 2.1 %collective-permute-done.10 = bf16[4,384,256]{2,1,0:T(8,128)(2,1)S(1)} collective-permute-done((bf16[4,384,256]{2,1,0:T(8,128)(2,1)}, bf16[4,384,256]{2,1,0:T(8,128)(2,1)S(1)}, u32[]{:S(2)}, u32[]{:S(2)}) %collective-permute-start.10) | collective-permute-done | bytes 786464 | tf_op jit(solution)/shard_map/ppermute | solution.py:34
  110.4 1.3 add_convert_fusion.1
  111.7 15.3 %all_to_all.20 = bf16[4,384,256]{2,1,0:T(8,128)(2,1)S(1)} all-to-all(bf16[4,384,256]{2,1,0:T(8,128)(2,1)S(1)} %add_convert_fusion.1), channel_id=1, replica_groups=mesh['rep'=2,'z'=4,'y'=8,'x'=4,'c'=2] {'x'}, dimensions={0} | all-to-all | bytes 1572864 | tf_op jit(solution)/shard_map/all_to_all | solution.py:26
  127.0 0.1 convert_reduce_fusion.1
  127.1 0.0 copy-start.8
  127.1 0.0 copy-start.9
  127.2 0.1 broadcast_in_dim.9
  127.2 13.0 %all_to_all.21.rows_ref = bf16[4,384,256]{2,1,0:T(8,128)(2,1)S(1)} all-to-all(bf16[4,384,256]{2,1,0:T(8,128)(2,1)S(1)} %broadcast_in_dim.9), channel_id=1, replica_groups=mesh['rep'=2,'z'=4,'y'=8,'x'=4,'c'=2] {'x'}, dimensions={0} | all-to-all | bytes 1572864 | tf_op jit(solution)/shard_map/all_to_all | solution.py:26
  140.3 4.5 %collective-permute-start.11 = (bf16[4,384,256]{2,1,0:T(8,128)(2,1)S(1)}, bf16[4,384,256]{2,1,0:T(8,128)(2,1)S(1)}, u32[]{:S(2)}, u32[]{:S(2)}) collective-permute-start(bf16[4,384,256]{2,1,0:T(8,128)(2,1)S(1)} %all_to_all.21.rows_ref), channel_id=1, source_target_pairs={{0,1},{1,0},{2,3},{3,2},{4,5},{5,4},{6,7},{7,6},{8,9},{9,8},{10,11... | collective-permute-start | bytes 2359304 | tf_op jit(solution)/shard_map/ppermute | solution.py:34
  144.8 0.6 reshape.28.gate_scale_ref
  145.4 0.6 reshape.29.up_scale_ref
  146.0 0.7 collective-permute-done.11.partner_ref
  146.7 0.9 copy-done.13
  147.6 9.5 %shard_map.174 = (bf16[4,384,256]{2,1,0:T(8,128)(2,1)}, bf16[4,384,256]{2,1,0:T(8,128)(2,1)}) custom-call(bf16[4,384,256]{2,1,0:T(8,128)(2,1)} %copy-done.3, bf16[4,384,256]{2,1,0:T(8,128)(2,1)} %copy-done.13, f32[4,2,1,256]{3,2,1,0:T(1,128)} %bitcast.24, f32[5,1,128]{2,1,0:T(1,128)} %reshape.28.gate_scale_ref, f32[5,1,128]{2,1,0:T(1,128)} %reshape.29.up_scale_ref, ...), custom_call_target="tpu_custom_call" | custom-call | flops 3019898880 | tf_op jit(solution)/shard_map/pallas_call | solution.py:300
  157.0 2.3 %collective-permute-start.12 = (bf16[4,384,256]{2,1,0:T(8,128)(2,1)}, bf16[4,384,256]{2,1,0:T(8,128)(2,1)S(1)}, u32[]{:S(2)}, u32[]{:S(2)}) collective-permute-start(bf16[4,384,256]{2,1,0:T(8,128)(2,1)} %get-tuple-element.12), channel_id=1, source_target_pairs={{0,1},{1,0},{2,3},{3,2},{4,5},{5,4},{6,7},{7,6},{8,9},{9,8},{10,11... | collective-permute-start | bytes 2359304 | tf_op jit(solution)/shard_map/ppermute | solution.py:34
  159.3 2.1 %collective-permute-done.12 = bf16[4,384,256]{2,1,0:T(8,128)(2,1)S(1)} collective-permute-done((bf16[4,384,256]{2,1,0:T(8,128)(2,1)}, bf16[4,384,256]{2,1,0:T(8,128)(2,1)S(1)}, u32[]{:S(2)}, u32[]{:S(2)}) %collective-permute-start.12) | collective-permute-done | bytes 786464 | tf_op jit(solution)/shard_map/ppermute | solution.py:34
  161.4 1.3 add_convert_fusion
  162.7 14.4 %all_to_all.22 = bf16[4,384,256]{2,1,0:T(8,128)(2,1)S(1)} all-to-all(bf16[4,384,256]{2,1,0:T(8,128)(2,1)S(1)} %add_convert_fusion), channel_id=1, replica_groups=mesh['rep'=2,'z'=4,'y'=8,'x'=4,'c'=2] {'x'}, dimensions={0} | all-to-all | bytes 1572864 | tf_op jit(solution)/shard_map/all_to_all | solution.py:26
  177.2 0.1 convert_reduce_fusion
  177.3 0.7 add_convert_fusion.2
  (23 shorter events, 0.1 us)
Async XLA Ops:
  6.5 140.1 %all-gather.2.cloned.1.call-start = ((), (), s32[]{:S(2)}) async-start(), calls=%async_computation.4 | async-start | bytes 8519680 | tf_op jit(solution)/shard_map/all_gather | solution.py:66
  9.3 10.6 %copy-start.4 = (bf16[384,256]{1,0:T(8,128)(2,1)S(1)}, bf16[384,256]{1,0:T(8,128)(2,1)}, u32[]{:S(2)}) copy-start(bf16[384,256]{1,0:T(8,128)(2,1)} %param.18) | copy-start | bytes 589828
  12.3 29.6 %all-to-all-start = ((bf16[8,2,64,384]{3,2,1,0:T(8,128)(2,1)}), bf16[8,2,64,384]{3,2,1,0:T(8,128)(2,1)S(1)}, u32[]{:S(2)}, u32[]{:S(2)}) async-start(bf16[8,2,64,384]{3,2,1,0:T(8,128)(2,1)} %broadcast_in_dim.8), calls=%async_computation | async-start | bytes 1572864 | tf_op jit(solution)/shard_map/all_to_all | solution.py:26
  19.9 10.0 %collective-permute-start = (bf16[384,256]{1,0:T(8,128)(2,1)S(1)}, bf16[384,256]{1,0:T(8,128)(2,1)S(1)}, u32[]{:S(2)}, u32[]{:S(2)}) collective-permute-start(bf16[384,256]{1,0:T(8,128)(2,1)S(1)} %copy-done.4), channel_id=1, source_target_pairs={{0,2},{2,4},{4,6},{6,0},{1,3},{3,5},{5,7},{7,1},{8,10},{10,12},{12... | collective-permute-start | bytes 589832 | tf_op jit(solution)/shard_map/ppermute | solution.py:43
  23.1 6.8 %collective-permute-start.1 = (bf16[384,256]{1,0:T(8,128)(2,1)S(1)}, bf16[384,256]{1,0:T(8,128)(2,1)S(1)}, u32[]{:S(2)}, u32[]{:S(2)}) collective-permute-start(bf16[384,256]{1,0:T(8,128)(2,1)S(1)} %copy-done.4), channel_id=1, source_target_pairs={{0,6},{2,0},{4,2},{6,4},{1,7},{3,1},{5,3},{7,5},{8,14},{10,8},{12,... | collective-permute-start | bytes 589832 | tf_op jit(solution)/shard_map/ppermute | solution.py:43
  26.5 8.2 %collective-permute-start.2 = (bf16[384,256]{1,0:T(8,128)(2,1)S(1)}, bf16[384,256]{1,0:T(8,128)(2,1)S(1)}, u32[]{:S(2)}, u32[]{:S(2)}) collective-permute-start(bf16[384,256]{1,0:T(8,128)(2,1)S(1)} %copy-done.4), channel_id=1, source_target_pairs={{0,4},{2,6},{4,0},{6,2},{1,5},{3,7},{5,1},{7,3},{8,12},{10,14},{12... | collective-permute-start | bytes 589832 | tf_op jit(solution)/shard_map/ppermute | solution.py:43
  34.7 40.4 %copy-start.12 = (f32[384]{0:T(512)S(1)}, f32[384]{0:T(512)}, u32[]{:S(2)}) copy-start(f32[384]{0:T(512)} %param.25) | copy-start | bytes 4612
  34.7 41.0 %copy-start.10 = (f32[384]{0:T(512)S(1)}, f32[384]{0:T(512)}, u32[]{:S(2)}) copy-start(f32[384]{0:T(512)} %param.21) | copy-start | bytes 4612
  34.7 41.6 %copy-start.11 = (f32[384]{0:T(512)S(1)}, f32[384]{0:T(512)}, u32[]{:S(2)}) copy-start(f32[384]{0:T(512)} %param.26) | copy-start | bytes 4612
  34.8 45.4 %copy-start = (bf16[4,384,256]{2,1,0:T(8,128)(2,1)}, bf16[4,384,256]{2,1,0:T(8,128)(2,1)S(1)}, u32[]{:S(2)}) copy-start(bf16[4,384,256]{2,1,0:T(8,128)(2,1)S(1)} %pad_maximum_fusion.rows_ref) | copy-start | bytes 2359300
  34.8 42.1 %collective-permute-start.3 = (bf16[4,384,256]{2,1,0:T(8,128)(2,1)S(1)}, bf16[4,384,256]{2,1,0:T(8,128)(2,1)S(1)}, u32[]{:S(2)}, u32[]{:S(2)}) collective-permute-start(bf16[4,384,256]{2,1,0:T(8,128)(2,1)S(1)} %pad_maximum_fusion.rows_ref), channel_id=1, source_target_pairs={{0,1},{1,0},{2,3},{3,2},{4,5},{5,4},{6,7},{7,6},{8,9},{9,8},{10,11... | collective-permute-start | bytes 2359304 | tf_op jit(solution)/shard_map/ppermute | solution.py:34
  42.8 37.4 %copy-start.1 = (bf16[8,1,64,384]{3,2,1,0:T(8,128)(2,1)}, bf16[8,1,64,384]{3,2,1,0:T(8,128)(2,1)S(1)}, u32[]{:S(2)}) copy-start(bf16[8,1,64,384]{3,2,1,0:T(8,128)(2,1)S(1)} %get-tuple-element.14) | copy-start | bytes 1179652
  42.8 23.8 %collective-permute-start.4 = (bf16[512,384]{1,0:T(8,128)(2,1)S(1)}, bf16[512,384]{1,0:T(8,128)(2,1)S(1)}, u32[]{:S(2)}, u32[]{:S(2)}) collective-permute-start(bf16[512,384]{1,0:T(8,128)(2,1)S(1)} %bitcast.16), channel_id=1, source_target_pairs={{0,64},{64,128},{128,192},{192,256},{256,320},{320,384},{384,448},... | collective-permute-start | bytes 1179656 | tf_op jit(solution)/shard_map/ppermute | solution.py:22
  50.0 20.4 %collective-permute-start.8 = (bf16[512,384]{1,0:T(8,128)(2,1)}, bf16[512,384]{1,0:T(8,128)(2,1)}, u32[]{:S(2)}, u32[]{:S(2)}) collective-permute-start(bf16[512,384]{1,0:T(8,128)(2,1)} %bitcast.9.own_ref), channel_id=1, source_target_pairs={{0,448},{64,0},{128,64},{192,128},{256,192},{320,256},{384,320},{4... | collective-permute-start | bytes 1179656 | tf_op jit(solution)/shard_map/ppermute | solution.py:22
  59.3 18.2 %collective-permute-start.5 = (bf16[512,384]{1,0:T(8,128)(2,1)S(1)}, bf16[512,384]{1,0:T(8,128)(2,1)S(1)}, u32[]{:S(2)}, u32[]{:S(2)}) collective-permute-start(bf16[512,384]{1,0:T(8,128)(2,1)S(1)} %bitcast.17), channel_id=1, source_target_pairs={{0,448},{64,0},{128,64},{192,128},{256,192},{320,256},{384,320},{4... | collective-permute-start | bytes 1179656 | tf_op jit(solution)/shard_map/ppermute | solution.py:22
  66.6 13.6 %copy-start.5 = (bf16[512,384]{1,0:T(8,128)(2,1)}, bf16[512,384]{1,0:T(8,128)(2,1)S(1)}, u32[]{:S(2)}) copy-start(bf16[512,384]{1,0:T(8,128)(2,1)S(1)} %collective-permute-done.4.before_ref) | copy-start | bytes 1179652
  66.6 13.6 %collective-permute-start.6 = (bf16[512,384]{1,0:T(8,128)(2,1)S(1)}, bf16[512,384]{1,0:T(8,128)(2,1)S(1)}, u32[]{:S(2)}, u32[]{:S(2)}) collective-permute-start(bf16[512,384]{1,0:T(8,128)(2,1)S(1)} %collective-permute-done.4.before_ref), channel_id=1, source_target_pairs={{0,64},{64,128},{128,192},{192,256},{256,320},{320,384},{384,448},... | collective-permute-start | bytes 1179656 | tf_op jit(solution)/shard_map/ppermute | solution.py:22
  68.5 28.5 %collective-permute-start.7 = (bf16[512,384]{1,0:T(8,128)(2,1)}, bf16[512,384]{1,0:T(8,128)(2,1)}, u32[]{:S(2)}, u32[]{:S(2)}) collective-permute-start(bf16[512,384]{1,0:T(8,128)(2,1)} %bitcast.9.own_ref), channel_id=1, source_target_pairs={{0,64},{64,128},{128,192},{192,256},{256,320},{320,384},{384,448},... | collective-permute-start | bytes 1179656 | tf_op jit(solution)/shard_map/ppermute | solution.py:22
  70.5 26.6 %collective-permute-start.9 = (bf16[512,384]{1,0:T(8,128)(2,1)}, bf16[512,384]{1,0:T(8,128)(2,1)}, u32[]{:S(2)}, u32[]{:S(2)}) collective-permute-start(bf16[512,384]{1,0:T(8,128)(2,1)} %collective-permute-done.8.after_ref), channel_id=1, source_target_pairs={{0,448},{64,0},{128,64},{192,128},{256,192},{320,256},{384,320},{4... | collective-permute-start | bytes 1179656 | tf_op jit(solution)/shard_map/ppermute | solution.py:22
  76.9 3.3 %copy-start.2 = (bf16[4,384,256]{2,1,0:T(8,128)(2,1)}, bf16[4,384,256]{2,1,0:T(8,128)(2,1)S(1)}, u32[]{:S(2)}) copy-start(bf16[4,384,256]{2,1,0:T(8,128)(2,1)S(1)} %collective-permute-done.3.partner_ref) | copy-start | bytes 2359300
  77.5 2.7 %copy-start.6 = (bf16[512,384]{1,0:T(8,128)(2,1)}, bf16[512,384]{1,0:T(8,128)(2,1)S(1)}, u32[]{:S(2)}) copy-start(bf16[512,384]{1,0:T(8,128)(2,1)S(1)} %collective-permute-done.5.after_ref) | copy-start | bytes 1179652
  80.2 0.8 copy-start.7
  100.3 10.0 %collective-permute-start.10 = (bf16[4,384,256]{2,1,0:T(8,128)(2,1)}, bf16[4,384,256]{2,1,0:T(8,128)(2,1)S(1)}, u32[]{:S(2)}, u32[]{:S(2)}) collective-permute-start(bf16[4,384,256]{2,1,0:T(8,128)(2,1)} %get-tuple-element.10), channel_id=1, source_target_pairs={{0,1},{1,0},{2,3},{3,2},{4,5},{5,4},{6,7},{7,6},{8,9},{9,8},{10,11... | collective-permute-start | bytes 2359304 | tf_op jit(solution)/shard_map/ppermute | solution.py:34
  127.1 17.7 %copy-start.8 = (f32[640]{0:T(1024)S(1)}, f32[640]{0:T(1024)}, u32[]{:S(2)}) copy-start(f32[640]{0:T(1024)} %param.31) | copy-start | bytes 7684
  127.1 18.3 %copy-start.9 = (f32[640]{0:T(1024)S(1)}, f32[640]{0:T(1024)}, u32[]{:S(2)}) copy-start(f32[640]{0:T(1024)} %param.33) | copy-start | bytes 7684
  140.3 6.4 %copy-start.3 = (bf16[4,384,256]{2,1,0:T(8,128)(2,1)}, bf16[4,384,256]{2,1,0:T(8,128)(2,1)S(1)}, u32[]{:S(2)}) copy-start(bf16[4,384,256]{2,1,0:T(8,128)(2,1)S(1)} %all_to_all.21.rows_ref) | copy-start | bytes 2359300
  140.3 6.4 %collective-permute-start.11 = (bf16[4,384,256]{2,1,0:T(8,128)(2,1)S(1)}, bf16[4,384,256]{2,1,0:T(8,128)(2,1)S(1)}, u32[]{:S(2)}, u32[]{:S(2)}) collective-permute-start(bf16[4,384,256]{2,1,0:T(8,128)(2,1)S(1)} %all_to_all.21.rows_ref), channel_id=1, source_target_pairs={{0,1},{1,0},{2,3},{3,2},{4,5},{5,4},{6,7},{7,6},{8,9},{9,8},{10,11... | collective-permute-start | bytes 2359304 | tf_op jit(solution)/shard_map/ppermute | solution.py:34
  146.7 0.9 copy-start.13
  157.0 4.4 %collective-permute-start.12 = (bf16[4,384,256]{2,1,0:T(8,128)(2,1)}, bf16[4,384,256]{2,1,0:T(8,128)(2,1)S(1)}, u32[]{:S(2)}, u32[]{:S(2)}) collective-permute-start(bf16[4,384,256]{2,1,0:T(8,128)(2,1)} %get-tuple-element.12), channel_id=1, source_target_pairs={{0,1},{1,0},{2,3},{3,2},{4,5},{5,4},{6,7},{7,6},{8,9},{9,8},{10,11... | collective-permute-start | bytes 2359304 | tf_op jit(solution)/shard_map/ppermute | solution.py:34
Sparse Core Ops, SparseCore 0:
  10.4 118.7 all-gather.1

commit v2 on v1

--- a/solution.py
+++ b/solution.py
@@ -92,6 +92,33 @@
 
 def halves(normed_ref, chip):
     return jnp.concatenate([normed_ref[chip, 0], normed_ref[chip, 1]], axis=1)
+
+
+def pack_kernel(rec_ref, mix_ref, scale_ref, out_hbm, both_ref, sems):
+    both_ref[0] = rec_ref[...].astype(BF16)
+    rows = mix_ref.shape[0]
+    scale = jnp.concatenate([scale_ref[...]] * (128 // rows), axis=1)
+    column = jnp.broadcast_to(scale, (128, 128)).T[:rows, :1]
+    both_ref[1] = (mix_ref[...] * column).astype(BF16)
+    copies = [
+        pltpu.make_async_copy(both_ref, out_hbm.at[i], sems.at[i]) for i in range(out_hbm.shape[0])
+    ]
+    for copy in copies:
+        copy.start()
+    for copy in copies:
+        copy.wait()
+
+
+def pack(rec, mix, scale, count):
+    rows, width = rec.shape
+    vmem = pl.BlockSpec(memory_space=pltpu.VMEM)
+    return pl.pallas_call(
+        pack_kernel,
+        out_shape=jax.ShapeDtypeStruct((count, 2, rows, width), BF16),
+        in_specs=[vmem] * 3,
+        out_specs=pl.BlockSpec(memory_space=pl.ANY),
+        scratch_shapes=[pltpu.VMEM((2, rows, width), BF16), pltpu.SemaphoreType.DMA((count,))],
+    )(rec, mix.T, scale.reshape(1, rows))
 
 
 def nearby(axis):
@@ -213,26 +240,23 @@
     sent_ref,
     out_sems,
     normed_ref,
-    in_ref,
-    out_ref,
+    weights_ref,
     sems,
 ):
-    width = in_ref.shape[2]
-    deep = in_ref.shape[1]
+    width = 128 * gate_scale_ref.shape[0]
+    deep = weights_ref.shape[1]
     step = deep // PIECES
     copies = []
-    for first, target in ((0, in_ref), (width, out_ref)):
-        for side in range(2):
-            for piece in range(PIECES):
-                span = pl.ds(side * deep + piece * step, step)
-                source = weights_hbm.at[span, pl.ds(first, target.shape[2])]
-                kept = target.at[side, pl.ds(piece * step, step)]
-                copy = pltpu.make_async_copy(source, kept, sems.at[len(copies)])
-                copy.start()
-                copies.append(copy)
-
-    def arrived(group):
-        for copy in copies[group * PIECES : (group + 1) * PIECES]:
+    for side in range(2):
+        for piece in range(PIECES):
+            source = weights_hbm.at[pl.ds(side * deep + piece * step, step)]
+            target = weights_ref.at[side, pl.ds(piece * step, step)]
+            copy = pltpu.make_async_copy(source, target, sems.at[len(copies)])
+            copy.start()
+            copies.append(copy)
+
+    def arrived(side):
+        for copy in copies[side * PIECES : (side + 1) * PIECES]:
             copy.wait()
 
     core = lax.axis_index("c")
@@ -242,20 +266,18 @@
     normalize(blocks, gain_ref, normed_ref)
     left = jnp.concatenate([halves(normed_ref, x) for x in range(chips)], axis=1)
     arrived(0)
-    gate = dot(left, in_ref[0]) * lanes(gate_scale_ref)
+    gate = dot(left, weights_ref[0, :, :width]) * lanes(gate_scale_ref)
     arrived(1)
-    up = dot(left, in_ref[1]) * lanes(up_scale_ref)
+    up = dot(left, weights_ref[1, :, :width]) * lanes(up_scale_ref)
     hidden = (gate * jax.nn.sigmoid(gate) * up).astype(BF16)
     first, second = hidden[:, : width // 2], hidden[:, width // 2 :]
-    arrived(2)
-    arrived(3)
     span = deep // chips
     out = Parts(kept_hbm, sent_hbm, kept_ref, sent_ref, out_sems)
     for x in range(chips):
 
         def product(rows):
-            one = dot_t(first, out_ref[0, rows])
-            return one + dot_t(second, out_ref[1, rows])
+            one = dot_t(first, weights_ref[0, rows, width:])
+            return one + dot_t(second, weights_ref[1, rows, width:])
 
         out.put(x, product, x * span)
     out.wait()
@@ -330,8 +352,6 @@
 ):
     rows, features = tokens.shape
     width = recurrent_input_weight.shape[1]
-    mix_rows = (mixing_output_weight * mixing_output_scale).T
-    pair = jnp.stack([recurrent_input_weight, mix_rows]).astype(BF16)
     down = (feedforward_down_weight * feedforward_down_scale).T
     half = down.shape[1] // 2
     ffn_blocks = over_plane(
@@ -339,12 +359,18 @@
         jnp.concatenate([feedforward_up_weight, down[:, half:]], axis=1),
     )
 
-    pair = copies_to(pair, "y")
+    copies = pack(
+        recurrent_input_weight, mixing_output_weight, mixing_output_scale, lax.axis_size("y")
+    )
+    pair = swap(copies, "y")
     rec_blocks = over_z(pair[:, 0].reshape(-1, width), 1)
     mix_blocks = over_z(pair[:, 1].reshape(-1, width), -1)
     rate = -DECAY_FACTOR * jax.nn.softplus(-channel_decay_parameter)
     count, size = recurrence_gate_weight_blocks.shape[:2]
-    tok = chips_from_here(tokens)
+    vectors = (recurrent_input_scale, rate, token_extra_log_decay)
+    vectors = [v.reshape(-1, 1, size) for v in vectors]
+    tok, scale, rate, extra = lax.optimization_barrier((tokens, *vectors))
+    tok = chips_from_here(tok)
     terms = [(4, rows, features)] * 2
     normed = pltpu.VMEM((4, 2, rows, features), BF16)
     (state,) = call(
@@ -354,12 +380,12 @@
             to_partner(tok),
             mixing_norm_gain.reshape(4, 2, 1, -1),
             *rec_blocks,
-            recurrent_input_scale.reshape(-1, 1, size),
+            scale,
             convolution_kernel_taps,
             recurrence_gate_weight_blocks,
             input_gate_weight_blocks,
-            rate.reshape(-1, 1, size),
-            token_extra_log_decay.reshape(-1, 1, size),
+            rate,
+            extra,
         ),
         (),
         [(rows, width)],
@@ -395,9 +421,8 @@
         terms,
         [
             normed,
-            pltpu.VMEM((2, 8 * features, hidden_width), BF16),
-            pltpu.VMEM((2, 8 * features, hidden_width // 2), BF16),
-            pltpu.SemaphoreType.DMA((4 * PIECES,)),
+            pltpu.VMEM((2, 8 * features, ffn_blocks.shape[1]), BF16),
+            pltpu.SemaphoreType.DMA((2 * PIECES,)),
         ],
         6 * rows * hidden_width * features * 8,
     )

time: 186 us -> 186 us (level)
  Pallas kernels: 18.7 us -> 21.1 us
  other arithmetic: 8.34 us -> 6.47 us
    ppermute x6, waiting for transfers between devices: 17.4 us -> 19.9 us  [shift_z(): lax.ppermute(value, ('rep', 'z'), [(i, (i + step) % count) for i in range...]
    pallas_call x0 -> x1, Pallas kernels: none -> 2.11 us  [pack(): pl.pallas_call(pack_kernel, out_shape=jax.ShapeDtypeStruct((count, 2, row...]
    another operation x3 -> x0, other arithmetic: 1.93 us -> none  [layer(): pair = jnp.stack([recurrent_input_weight, mix_rows]).astype(BF16)]
  transfers between devices with their start and end apart: 15 -> 15, of which waited for: 9 -> 8; matrix products, arithmetic and copies ran while one was open for 5% -> 3% of each run, Pallas kernels for 5% -> 6%
where the time goes in v2:
time: 186 us; the launch traced here: 185 us
  starting transfers between devices  64.9 us (35%)
  blocking collectives  42.7 us (23%)
  waiting for transfers between devices  29.6 us (16%)
  Pallas kernels  21.1 us (11%)
  between operations  13.8 us (7%)
  other arithmetic  6.47 us (3%)
  local copies, waits for them, and re-layouts  6.31 us (3%)
    all_to_all x3, blocking collectives, swap(): return lax.all_to_all(value, axis, split_axis=0, concat_axis=0, tiled=True)  42.7 us
    ppermute x6, starting transfers between devices, shift_z(): lax.ppermute(value, ('rep', 'z'), [(i, (i + step) % count) for i in range...  27.8 us
    ppermute x6, waiting for transfers between devices, shift_z(): lax.ppermute(value, ('rep', 'z'), [(i, (i + step) % count) for i in range...  19.9 us
    ppermute x4, starting transfers between devices, to_partner(): return lax.ppermute(value, 'c', [(0, 1), (1, 0)])  19.5 us
    pallas_call x3, Pallas kernels, call(): pl.pallas_call(kernel, out_shape=[jax.ShapeDtypeStruct(shape, BF16) for s...  19 us
    ppermute x3, starting transfers between devices, shift_x(): lax.ppermute(value, 'x', [(i, (i + step) % count) for i in range(count)])  9.92 us
    all_to_all x1, starting transfers between devices, swap(): return lax.all_to_all(value, axis, split_axis=0, concat_axis=0, tiled=True)  7.65 us
    ppermute x4, waiting for transfers between devices, to_partner(): return lax.ppermute(value, 'c', [(0, 1), (1, 0)])  4.93 us
  transfers between devices with their start and end apart: 15, of which 8 were waited for; matrix products, arithmetic and copies ran while one was open for 3% of the time, Pallas kernels for 6%

profile of v2, /device:TPU:1, one launch (start us, length us, event | category | flops | bytes accessed | tf_op | source)
XLA Modules:
  0.0 184.9 jit_solution(560688219617967469)
XLA Ops:
  6.5 1.0 multiply_bitcast_fusion
  7.5 0.1 fusion.3
  7.6 0.0 copy-start.13
  7.6 0.0 copy-start.11
  7.7 0.0 copy-start.12
  7.7 0.0 copy-start.4
  7.7 1.7 fusion
  9.4 0.0 all-gather.2.cloned.1.call-update
  9.4 2.1 %shard_map.172 = bf16[8,2,64,384]{3,2,1,0:T(8,128)(2,1)} custom-call(f32[64,384]{1,0:T(8,128)} %rec_ref.1, f32[64,384]{1,0:T(8,128)} %bitcast.22, f32[1,64]{1,0:T(1,128)} %bitcast.24), custom_call_target="tpu_custom_call" | custom-call | tf_op jit(solution)/shard_map/pallas_call | solution.py:115
  11.5 7.7 %all-to-all-start = ((bf16[8,2,64,384]{3,2,1,0:T(8,128)(2,1)}), bf16[8,2,64,384]{3,2,1,0:T(8,128)(2,1)S(1)}, u32[]{:S(2)}, u32[]{:S(2)}) async-start(bf16[8,2,64,384]{3,2,1,0:T(8,128)(2,1)} %shard_map.172), calls=%async_computation | async-start | bytes 1572864 | tf_op jit(solution)/shard_map/all_to_all | solution.py:26
  19.2 0.6 reshape.26.rate_ref
  19.8 0.6 reshape.25.scale_ref
  20.4 0.6 reshape.27.extra_ref
  21.0 3.1 %collective-permute-start = (bf16[384,256]{1,0:T(8,128)(2,1)S(1)}, bf16[384,256]{1,0:T(8,128)(2,1)S(1)}, u32[]{:S(2)}, u32[]{:S(2)}) collective-permute-start(bf16[384,256]{1,0:T(8,128)(2,1)S(1)} %copy-done.4), channel_id=1, source_target_pairs={{0,2},{2,4},{4,6},{6,0},{1,3},{3,5},{5,7},{7,1},{8,10},{10,12},{12... | collective-permute-start | bytes 589832 | tf_op jit(solution)/shard_map/ppermute | solution.py:43
  24.2 3.4 %collective-permute-start.1 = (bf16[384,256]{1,0:T(8,128)(2,1)S(1)}, bf16[384,256]{1,0:T(8,128)(2,1)S(1)}, u32[]{:S(2)}, u32[]{:S(2)}) collective-permute-start(bf16[384,256]{1,0:T(8,128)(2,1)S(1)} %copy-done.4), channel_id=1, source_target_pairs={{0,6},{2,0},{4,2},{6,4},{1,7},{3,1},{5,3},{7,5},{8,14},{10,8},{12,... | collective-permute-start | bytes 589832 | tf_op jit(solution)/shard_map/ppermute | solution.py:43
  27.5 3.4 %collective-permute-start.2 = (bf16[384,256]{1,0:T(8,128)(2,1)S(1)}, bf16[384,256]{1,0:T(8,128)(2,1)S(1)}, u32[]{:S(2)}, u32[]{:S(2)}) collective-permute-start(bf16[384,256]{1,0:T(8,128)(2,1)S(1)} %copy-done.4), channel_id=1, source_target_pairs={{0,4},{2,6},{4,0},{6,2},{1,5},{3,7},{5,1},{7,3},{8,12},{10,14},{12... | collective-permute-start | bytes 589832 | tf_op jit(solution)/shard_map/ppermute | solution.py:43
  31.0 0.0 collective-permute-done
  31.0 0.0 collective-permute-done.1
  31.0 4.7 %collective-permute-done.2 = bf16[384,256]{1,0:T(8,128)(2,1)S(1)} collective-permute-done((bf16[384,256]{1,0:T(8,128)(2,1)S(1)}, bf16[384,256]{1,0:T(8,128)(2,1)S(1)}, u32[]{:S(2)}, u32[]{:S(2)}) %collective-permute-start.2) | collective-permute-done | bytes 196640 | tf_op jit(solution)/shard_map/ppermute | solution.py:43
  35.8 0.1 pad_maximum_fusion.rows_ref
  35.9 6.1 %collective-permute-start.3 = (bf16[4,384,256]{2,1,0:T(8,128)(2,1)S(1)}, bf16[4,384,256]{2,1,0:T(8,128)(2,1)S(1)}, u32[]{:S(2)}, u32[]{:S(2)}) collective-permute-start(bf16[4,384,256]{2,1,0:T(8,128)(2,1)S(1)} %pad_maximum_fusion.rows_ref), channel_id=1, source_target_pairs={{0,1},{1,0},{2,3},{3,2},{4,5},{5,4},{6,7},{7,6},{8,9},{9,8},{10,11... | collective-permute-start | bytes 2359304 | tf_op jit(solution)/shard_map/ppermute | solution.py:34
  42.0 0.0 all-to-all-done
  42.0 0.1 fusion.2
  42.1 0.0 copy-start.1
  42.1 0.0 copy-start.8
  42.1 6.3 %collective-permute-start.4 = (bf16[512,384]{1,0:T(8,128)(2,1)S(1)}, bf16[512,384]{1,0:T(8,128)(2,1)S(1)}, u32[]{:S(2)}, u32[]{:S(2)}) collective-permute-start(bf16[512,384]{1,0:T(8,128)(2,1)S(1)} %bitcast.12), channel_id=1, source_target_pairs={{0,64},{64,128},{128,192},{192,256},{256,320},{320,384},{384,448},... | collective-permute-start | bytes 1179656 | tf_op jit(solution)/shard_map/ppermute | solution.py:22
  48.4 9.7 %collective-permute-start.8 = (bf16[512,384]{1,0:T(8,128)(2,1)S(1)}, bf16[512,384]{1,0:T(8,128)(2,1)S(1)}, u32[]{:S(2)}, u32[]{:S(2)}) collective-permute-start(bf16[512,384]{1,0:T(8,128)(2,1)S(1)} %bitcast.16), channel_id=1, source_target_pairs={{0,448},{64,0},{128,64},{192,128},{256,192},{320,256},{384,320},{4... | collective-permute-start | bytes 1179656 | tf_op jit(solution)/shard_map/ppermute | solution.py:22
  58.1 3.4 %collective-permute-start.5 = (bf16[512,384]{1,0:T(8,128)(2,1)S(1)}, bf16[512,384]{1,0:T(8,128)(2,1)S(1)}, u32[]{:S(2)}, u32[]{:S(2)}) collective-permute-start(bf16[512,384]{1,0:T(8,128)(2,1)S(1)} %bitcast.13), channel_id=1, source_target_pairs={{0,448},{64,0},{128,64},{192,128},{256,192},{320,256},{384,320},{4... | collective-permute-start | bytes 1179656 | tf_op jit(solution)/shard_map/ppermute | solution.py:22
  61.5 4.6 %collective-permute-done.4.before_ref = bf16[512,384]{1,0:T(8,128)(2,1)S(1)} collective-permute-done((bf16[512,384]{1,0:T(8,128)(2,1)S(1)}, bf16[512,384]{1,0:T(8,128)(2,1)S(1)}, u32[]{:S(2)}, u32[]{:S(2)}) %collective-permute-start.4) | collective-permute-done | bytes 393248 | tf_op jit(solution)/shard_map/ppermute | solution.py:22
  66.1 1.9 %collective-permute-start.6 = (bf16[512,384]{1,0:T(8,128)(2,1)S(1)}, bf16[512,384]{1,0:T(8,128)(2,1)S(1)}, u32[]{:S(2)}, u32[]{:S(2)}) collective-permute-start(bf16[512,384]{1,0:T(8,128)(2,1)S(1)} %collective-permute-done.4.before_ref), channel_id=1, source_target_pairs={{0,64},{64,128},{128,192},{192,256},{256,320},{320,384},{384,448},... | collective-permute-start | bytes 1179656 | tf_op jit(solution)/shard_map/ppermute | solution.py:22
  68.0 1.9 %collective-permute-start.7 = (bf16[512,384]{1,0:T(8,128)(2,1)S(1)}, bf16[512,384]{1,0:T(8,128)(2,1)S(1)}, u32[]{:S(2)}, u32[]{:S(2)}) collective-permute-start(bf16[512,384]{1,0:T(8,128)(2,1)S(1)} %bitcast.17), channel_id=1, source_target_pairs={{0,64},{64,128},{128,192},{192,256},{256,320},{320,384},{384,448},... | collective-permute-start | bytes 1179656 | tf_op jit(solution)/shard_map/ppermute | solution.py:22
  69.9 0.0 collective-permute-done.8.after_ref
  69.9 4.6 %collective-permute-start.9 = (bf16[512,384]{1,0:T(8,128)(2,1)S(1)}, bf16[512,384]{1,0:T(8,128)(2,1)S(1)}, u32[]{:S(2)}, u32[]{:S(2)}) collective-permute-start(bf16[512,384]{1,0:T(8,128)(2,1)S(1)} %collective-permute-done.8.after_ref), channel_id=1, source_target_pairs={{0,448},{64,0},{128,64},{192,128},{256,192},{320,256},{384,320},{4... | collective-permute-start | bytes 1179656 | tf_op jit(solution)/shard_map/ppermute | solution.py:22
  74.5 0.0 collective-permute-done.3.partner_ref
  74.5 1.0 collective-permute-done.5.after_ref
  75.6 4.2 %collective-permute-done.6.far_ref = bf16[512,384]{1,0:T(8,128)(2,1)S(1)} collective-permute-done((bf16[512,384]{1,0:T(8,128)(2,1)S(1)}, bf16[512,384]{1,0:T(8,128)(2,1)S(1)}, u32[]{:S(2)}, u32[]{:S(2)}) %collective-permute-start.6) | collective-permute-done | bytes 393248 | tf_op jit(solution)/shard_map/ppermute | solution.py:22
  79.8 0.7 copy-done.7
  80.5 6.0 %shard_map.173.state_ref = bf16[384,384]{1,0:T(8,128)(2,1)} custom-call(bf16[4,384,256]{2,1,0:T(8,128)(2,1)} %copy-done, bf16[4,384,256]{2,1,0:T(8,128)(2,1)} %copy-done.2, f32[4,2,1,256]{3,2,1,0:T(1,128)} %bitcast.23, bf16[512,384]{1,0:T(8,128)(2,1)} %bitcast.14, bf16[512,384]{1,0:T(8,128)(2,1)} %copy-done.5, bf16[512,384]{1,0:T(8,128)(2,1)} %copy-done.6, ...), custom_call_target="tpu_custom_call" | custom-call | flops 603979776 | tf_op jit(solution)/shard_map/pallas_call | solution.py:322
  86.5 10.1 %collective-permute-done.7.before_ref = bf16[512,384]{1,0:T(8,128)(2,1)S(1)} collective-permute-done((bf16[512,384]{1,0:T(8,128)(2,1)S(1)}, bf16[512,384]{1,0:T(8,128)(2,1)S(1)}, u32[]{:S(2)}, u32[]{:S(2)}) %collective-permute-start.7) | collective-permute-done | bytes 393248 | tf_op jit(solution)/shard_map/ppermute | solution.py:22
  96.6 0.0 collective-permute-done.9.far_ref
  96.6 0.7 copy-done.16
  97.3 0.7 copy-done.17
  98.1 3.3 %shard_map.174 = (bf16[4,384,256]{2,1,0:T(8,128)(2,1)}, bf16[4,384,256]{2,1,0:T(8,128)(2,1)}) custom-call(bf16[384,384]{1,0:T(8,128)(2,1)} %shard_map.173.state_ref, bf16[512,384]{1,0:T(8,128)(2,1)} %bitcast.18, bf16[512,384]{1,0:T(8,128)(2,1)} %copy-done.16, bf16[512,384]{1,0:T(8,128)(2,1)} %copy-done.15, bf16[512,384]{1,0:T(8,128)(2,1)} %copy-done.17), custom_call_target="tpu_custom_call" | custom-call | flops 603979776 | tf_op jit(solution)/shard_map/pallas_call | solution.py:322
  101.4 6.7 %collective-permute-start.10 = (bf16[4,384,256]{2,1,0:T(8,128)(2,1)}, bf16[4,384,256]{2,1,0:T(8,128)(2,1)S(1)}, u32[]{:S(2)}, u32[]{:S(2)}) collective-permute-start(bf16[4,384,256]{2,1,0:T(8,128)(2,1)} %get-tuple-element.18), channel_id=1, source_target_pairs={{0,1},{1,0},{2,3},{3,2},{4,5},{5,4},{6,7},{7,6},{8,9},{9,8},{10,11... | collective-permute-start | bytes 2359304 | tf_op jit(solution)/shard_map/ppermute | solution.py:34
  108.1 2.1 %collective-permute-done.10 = bf16[4,384,256]{2,1,0:T(8,128)(2,1)S(1)} collective-permute-done((bf16[4,384,256]{2,1,0:T(8,128)(2,1)}, bf16[4,384,256]{2,1,0:T(8,128)(2,1)S(1)}, u32[]{:S(2)}, u32[]{:S(2)}) %collective-permute-start.10) | collective-permute-done | bytes 786464 | tf_op jit(solution)/shard_map/ppermute | solution.py:34
  110.2 1.4 add_convert_fusion.1
  111.6 15.2 %all_to_all.20 = bf16[4,384,256]{2,1,0:T(8,128)(2,1)S(1)} all-to-all(bf16[4,384,256]{2,1,0:T(8,128)(2,1)S(1)} %add_convert_fusion.1), channel_id=1, replica_groups=mesh['rep'=2,'z'=4,'y'=8,'x'=4,'c'=2] {'x'}, dimensions={0} | all-to-all | bytes 1572864 | tf_op jit(solution)/shard_map/all_to_all | solution.py:26
  126.8 0.1 convert_reduce_fusion.1
  126.9 0.0 copy-start.9
  126.9 0.0 copy-start.10
  127.0 0.1 broadcast_in_dim.4
  127.0 13.1 %all_to_all.21.rows_ref = bf16[4,384,256]{2,1,0:T(8,128)(2,1)S(1)} all-to-all(bf16[4,384,256]{2,1,0:T(8,128)(2,1)S(1)} %broadcast_in_dim.4), channel_id=1, replica_groups=mesh['rep'=2,'z'=4,'y'=8,'x'=4,'c'=2] {'x'}, dimensions={0} | all-to-all | bytes 1572864 | tf_op jit(solution)/shard_map/all_to_all | solution.py:26
  140.1 4.5 %collective-permute-start.11 = (bf16[4,384,256]{2,1,0:T(8,128)(2,1)S(1)}, bf16[4,384,256]{2,1,0:T(8,128)(2,1)S(1)}, u32[]{:S(2)}, u32[]{:S(2)}) collective-permute-start(bf16[4,384,256]{2,1,0:T(8,128)(2,1)S(1)} %all_to_all.21.rows_ref), channel_id=1, source_target_pairs={{0,1},{1,0},{2,3},{3,2},{4,5},{5,4},{6,7},{7,6},{8,9},{9,8},{10,11... | collective-permute-start | bytes 2359304 | tf_op jit(solution)/shard_map/ppermute | solution.py:34
  144.6 0.6 reshape.31.gate_scale_ref
  145.2 0.5 reshape.32.up_scale_ref
  145.8 0.7 collective-permute-done.11.partner_ref
  146.5 0.9 copy-done.14
  147.4 9.8 %shard_map.175 = (bf16[4,384,256]{2,1,0:T(8,128)(2,1)}, bf16[4,384,256]{2,1,0:T(8,128)(2,1)}) custom-call(bf16[4,384,256]{2,1,0:T(8,128)(2,1)} %copy-done.3, bf16[4,384,256]{2,1,0:T(8,128)(2,1)} %copy-done.14, f32[4,2,1,256]{3,2,1,0:T(1,128)} %bitcast.25, f32[5,1,128]{2,1,0:T(1,128)} %reshape.31.gate_scale_ref, f32[5,1,128]{2,1,0:T(1,128)} %reshape.32.up_scale_ref, ...), custom_call_target="tpu_custom_call" | custom-call | flops 3019898880 | tf_op jit(solution)/shard_map/pallas_call | solution.py:322
  157.1 2.3 %collective-permute-start.12 = (bf16[4,384,256]{2,1,0:T(8,128)(2,1)}, bf16[4,384,256]{2,1,0:T(8,128)(2,1)S(1)}, u32[]{:S(2)}, u32[]{:S(2)}) collective-permute-start(bf16[4,384,256]{2,1,0:T(8,128)(2,1)} %get-tuple-element.20), channel_id=1, source_target_pairs={{0,1},{1,0},{2,3},{3,2},{4,5},{5,4},{6,7},{7,6},{8,9},{9,8},{10,11... | collective-permute-start | bytes 2359304 | tf_op jit(solution)/shard_map/ppermute | solution.py:34
  159.4 2.1 %collective-permute-done.12 = bf16[4,384,256]{2,1,0:T(8,128)(2,1)S(1)} collective-permute-done((bf16[4,384,256]{2,1,0:T(8,128)(2,1)}, bf16[4,384,256]{2,1,0:T(8,128)(2,1)S(1)}, u32[]{:S(2)}, u32[]{:S(2)}) %collective-permute-start.12) | collective-permute-done | bytes 786464 | tf_op jit(solution)/shard_map/ppermute | solution.py:34
  161.5 1.3 add_convert_fusion
  162.8 14.4 %all_to_all.22 = bf16[4,384,256]{2,1,0:T(8,128)(2,1)S(1)} all-to-all(bf16[4,384,256]{2,1,0:T(8,128)(2,1)S(1)} %add_convert_fusion), channel_id=1, replica_groups=mesh['rep'=2,'z'=4,'y'=8,'x'=4,'c'=2] {'x'}, dimensions={0} | all-to-all | bytes 1572864 | tf_op jit(solution)/shard_map/all_to_all | solution.py:26
  177.3 0.1 convert_reduce_fusion
  177.4 0.7 add_convert_fusion.2
  (28 shorter events, 0.1 us)
Async XLA Ops:
  6.5 140.0 %all-gather.2.cloned.1.call-start = ((), (), s32[]{:S(2)}) async-start(), calls=%async_computation.4 | async-start | bytes 8519680 | tf_op jit(solution)/shard_map/all_gather | solution.py:66
  7.6 11.6 %copy-start.13 = (f32[384]{0:T(512)S(1)}, f32[384]{0:T(512)}, u32[]{:S(2)}) copy-start(f32[384]{0:T(512)} %param.25) | copy-start | bytes 4612
  7.6 12.2 %copy-start.11 = (f32[384]{0:T(512)S(1)}, f32[384]{0:T(512)}, u32[]{:S(2)}) copy-start(f32[384]{0:T(512)} %param.21) | copy-start | bytes 4612
  7.7 12.8 %copy-start.12 = (f32[384]{0:T(512)S(1)}, f32[384]{0:T(512)}, u32[]{:S(2)}) copy-start(f32[384]{0:T(512)} %param.26) | copy-start | bytes 4612
  7.7 13.4 %copy-start.4 = (bf16[384,256]{1,0:T(8,128)(2,1)S(1)}, bf16[384,256]{1,0:T(8,128)(2,1)}, u32[]{:S(2)}) copy-start(bf16[384,256]{1,0:T(8,128)(2,1)} %param.18) | copy-start | bytes 589828
  11.5 30.4 %all-to-all-start = ((bf16[8,2,64,384]{3,2,1,0:T(8,128)(2,1)}), bf16[8,2,64,384]{3,2,1,0:T(8,128)(2,1)S(1)}, u32[]{:S(2)}, u32[]{:S(2)}) async-start(bf16[8,2,64,384]{3,2,1,0:T(8,128)(2,1)} %shard_map.172), calls=%async_computation | async-start | bytes 1572864 | tf_op jit(solution)/shard_map/all_to_all | solution.py:26
  21.0 9.9 %collective-permute-start = (bf16[384,256]{1,0:T(8,128)(2,1)S(1)}, bf16[384,256]{1,0:T(8,128)(2,1)S(1)}, u32[]{:S(2)}, u32[]{:S(2)}) collective-permute-start(bf16[384,256]{1,0:T(8,128)(2,1)S(1)} %copy-done.4), channel_id=1, source_target_pairs={{0,2},{2,4},{4,6},{6,0},{1,3},{3,5},{5,7},{7,1},{8,10},{10,12},{12... | collective-permute-start | bytes 589832 | tf_op jit(solution)/shard_map/ppermute | solution.py:43
  24.2 6.8 %collective-permute-start.1 = (bf16[384,256]{1,0:T(8,128)(2,1)S(1)}, bf16[384,256]{1,0:T(8,128)(2,1)S(1)}, u32[]{:S(2)}, u32[]{:S(2)}) collective-permute-start(bf16[384,256]{1,0:T(8,128)(2,1)S(1)} %copy-done.4), channel_id=1, source_target_pairs={{0,6},{2,0},{4,2},{6,4},{1,7},{3,1},{5,3},{7,5},{8,14},{10,8},{12,... | collective-permute-start | bytes 589832 | tf_op jit(solution)/shard_map/ppermute | solution.py:43
  27.5 8.2 %collective-permute-start.2 = (bf16[384,256]{1,0:T(8,128)(2,1)S(1)}, bf16[384,256]{1,0:T(8,128)(2,1)S(1)}, u32[]{:S(2)}, u32[]{:S(2)}) collective-permute-start(bf16[384,256]{1,0:T(8,128)(2,1)S(1)} %copy-done.4), channel_id=1, source_target_pairs={{0,4},{2,6},{4,0},{6,2},{1,5},{3,7},{5,1},{7,3},{8,12},{10,14},{12... | collective-permute-start | bytes 589832 | tf_op jit(solution)/shard_map/ppermute | solution.py:43
  35.9 43.9 %copy-start = (bf16[4,384,256]{2,1,0:T(8,128)(2,1)}, bf16[4,384,256]{2,1,0:T(8,128)(2,1)S(1)}, u32[]{:S(2)}) copy-start(bf16[4,384,256]{2,1,0:T(8,128)(2,1)S(1)} %pad_maximum_fusion.rows_ref) | copy-start | bytes 2359300
  35.9 38.7 %collective-permute-start.3 = (bf16[4,384,256]{2,1,0:T(8,128)(2,1)S(1)}, bf16[4,384,256]{2,1,0:T(8,128)(2,1)S(1)}, u32[]{:S(2)}, u32[]{:S(2)}) collective-permute-start(bf16[4,384,256]{2,1,0:T(8,128)(2,1)S(1)} %pad_maximum_fusion.rows_ref), channel_id=1, source_target_pairs={{0,1},{1,0},{2,3},{3,2},{4,5},{5,4},{6,7},{7,6},{8,9},{9,8},{10,11... | collective-permute-start | bytes 2359304 | tf_op jit(solution)/shard_map/ppermute | solution.py:34
  42.1 37.7 %copy-start.1 = (bf16[8,1,64,384]{3,2,1,0:T(8,128)(2,1)}, bf16[8,1,64,384]{3,2,1,0:T(8,128)(2,1)S(1)}, u32[]{:S(2)}) copy-start(bf16[8,1,64,384]{3,2,1,0:T(8,128)(2,1)S(1)} %get-tuple-element.22) | copy-start | bytes 1179652
  42.1 54.5 %copy-start.8 = (bf16[8,1,64,384]{3,2,1,0:T(8,128)(2,1)}, bf16[8,1,64,384]{3,2,1,0:T(8,128)(2,1)S(1)}, u32[]{:S(2)}) copy-start(bf16[8,1,64,384]{3,2,1,0:T(8,128)(2,1)S(1)} %get-tuple-element.21) | copy-start | bytes 1179652
  42.1 24.0 %collective-permute-start.4 = (bf16[512,384]{1,0:T(8,128)(2,1)S(1)}, bf16[512,384]{1,0:T(8,128)(2,1)S(1)}, u32[]{:S(2)}, u32[]{:S(2)}) collective-permute-start(bf16[512,384]{1,0:T(8,128)(2,1)S(1)} %bitcast.12), channel_id=1, source_target_pairs={{0,64},{64,128},{128,192},{192,256},{256,320},{320,384},{384,448},... | collective-permute-start | bytes 1179656 | tf_op jit(solution)/shard_map/ppermute | solution.py:22
  48.4 21.6 %collective-permute-start.8 = (bf16[512,384]{1,0:T(8,128)(2,1)S(1)}, bf16[512,384]{1,0:T(8,128)(2,1)S(1)}, u32[]{:S(2)}, u32[]{:S(2)}) collective-permute-start(bf16[512,384]{1,0:T(8,128)(2,1)S(1)} %bitcast.16), channel_id=1, source_target_pairs={{0,448},{64,0},{128,64},{192,128},{256,192},{320,256},{384,320},{4... | collective-permute-start | bytes 1179656 | tf_op jit(solution)/shard_map/ppermute | solution.py:22
  58.1 17.4 %collective-permute-start.5 = (bf16[512,384]{1,0:T(8,128)(2,1)S(1)}, bf16[512,384]{1,0:T(8,128)(2,1)S(1)}, u32[]{:S(2)}, u32[]{:S(2)}) collective-permute-start(bf16[512,384]{1,0:T(8,128)(2,1)S(1)} %bitcast.13), channel_id=1, source_target_pairs={{0,448},{64,0},{128,64},{192,128},{256,192},{320,256},{384,320},{4... | collective-permute-start | bytes 1179656 | tf_op jit(solution)/shard_map/ppermute | solution.py:22
  66.1 13.7 %copy-start.5 = (bf16[512,384]{1,0:T(8,128)(2,1)}, bf16[512,384]{1,0:T(8,128)(2,1)S(1)}, u32[]{:S(2)}) copy-start(bf16[512,384]{1,0:T(8,128)(2,1)S(1)} %collective-permute-done.4.before_ref) | copy-start | bytes 1179652
  66.1 13.7 %collective-permute-start.6 = (bf16[512,384]{1,0:T(8,128)(2,1)S(1)}, bf16[512,384]{1,0:T(8,128)(2,1)S(1)}, u32[]{:S(2)}, u32[]{:S(2)}) collective-permute-start(bf16[512,384]{1,0:T(8,128)(2,1)S(1)} %collective-permute-done.4.before_ref), channel_id=1, source_target_pairs={{0,64},{64,128},{128,192},{192,256},{256,320},{320,384},{384,448},... | collective-permute-start | bytes 1179656 | tf_op jit(solution)/shard_map/ppermute | solution.py:22
  68.0 28.6 %collective-permute-start.7 = (bf16[512,384]{1,0:T(8,128)(2,1)S(1)}, bf16[512,384]{1,0:T(8,128)(2,1)S(1)}, u32[]{:S(2)}, u32[]{:S(2)}) collective-permute-start(bf16[512,384]{1,0:T(8,128)(2,1)S(1)} %bitcast.17), channel_id=1, source_target_pairs={{0,64},{64,128},{128,192},{192,256},{256,320},{320,384},{384,448},... | collective-permute-start | bytes 1179656 | tf_op jit(solution)/shard_map/ppermute | solution.py:22
  69.9 26.7 %copy-start.15 = (bf16[512,384]{1,0:T(8,128)(2,1)}, bf16[512,384]{1,0:T(8,128)(2,1)S(1)}, u32[]{:S(2)}) copy-start(bf16[512,384]{1,0:T(8,128)(2,1)S(1)} %collective-permute-done.8.after_ref) | copy-start | bytes 1179652
  69.9 26.7 %collective-permute-start.9 = (bf16[512,384]{1,0:T(8,128)(2,1)S(1)}, bf16[512,384]{1,0:T(8,128)(2,1)S(1)}, u32[]{:S(2)}, u32[]{:S(2)}) collective-permute-start(bf16[512,384]{1,0:T(8,128)(2,1)S(1)} %collective-permute-done.8.after_ref), channel_id=1, source_target_pairs={{0,448},{64,0},{128,64},{192,128},{256,192},{320,256},{384,320},{4... | collective-permute-start | bytes 1179656 | tf_op jit(solution)/shard_map/ppermute | solution.py:22
  74.5 5.2 %copy-start.2 = (bf16[4,384,256]{2,1,0:T(8,128)(2,1)}, bf16[4,384,256]{2,1,0:T(8,128)(2,1)S(1)}, u32[]{:S(2)}) copy-start(bf16[4,384,256]{2,1,0:T(8,128)(2,1)S(1)} %collective-permute-done.3.partner_ref) | copy-start | bytes 2359300
  75.6 4.2 %copy-start.6 = (bf16[512,384]{1,0:T(8,128)(2,1)}, bf16[512,384]{1,0:T(8,128)(2,1)S(1)}, u32[]{:S(2)}) copy-start(bf16[512,384]{1,0:T(8,128)(2,1)S(1)} %collective-permute-done.5.after_ref) | copy-start | bytes 1179652
  79.8 0.8 copy-start.7
  96.6 0.7 copy-start.16
  97.3 0.7 copy-start.17
  101.4 8.8 %collective-permute-start.10 = (bf16[4,384,256]{2,1,0:T(8,128)(2,1)}, bf16[4,384,256]{2,1,0:T(8,128)(2,1)S(1)}, u32[]{:S(2)}, u32[]{:S(2)}) collective-permute-start(bf16[4,384,256]{2,1,0:T(8,128)(2,1)} %get-tuple-element.18), channel_id=1, source_target_pairs={{0,1},{1,0},{2,3},{3,2},{4,5},{5,4},{6,7},{7,6},{8,9},{9,8},{10,11... | collective-permute-start | bytes 2359304 | tf_op jit(solution)/shard_map/ppermute | solution.py:34
  126.9 17.7 %copy-start.9 = (f32[640]{0:T(1024)S(1)}, f32[640]{0:T(1024)}, u32[]{:S(2)}) copy-start(f32[640]{0:T(1024)} %param.31) | copy-start | bytes 7684
  126.9 18.3 %copy-start.10 = (f32[640]{0:T(1024)S(1)}, f32[640]{0:T(1024)}, u32[]{:S(2)}) copy-start(f32[640]{0:T(1024)} %param.33) | copy-start | bytes 7684
  140.1 6.4 %copy-start.3 = (bf16[4,384,256]{2,1,0:T(8,128)(2,1)}, bf16[4,384,256]{2,1,0:T(8,128)(2,1)S(1)}, u32[]{:S(2)}) copy-start(bf16[4,384,256]{2,1,0:T(8,128)(2,1)S(1)} %all_to_all.21.rows_ref) | copy-start | bytes 2359300
  140.1 6.4 %collective-permute-start.11 = (bf16[4,384,256]{2,1,0:T(8,128)(2,1)S(1)}, bf16[4,384,256]{2,1,0:T(8,128)(2,1)S(1)}, u32[]{:S(2)}, u32[]{:S(2)}) collective-permute-start(bf16[4,384,256]{2,1,0:T(8,128)(2,1)S(1)} %all_to_all.21.rows_ref), channel_id=1, source_target_pairs={{0,1},{1,0},{2,3},{3,2},{4,5},{5,4},{6,7},{7,6},{8,9},{9,8},{10,11... | collective-permute-start | bytes 2359304 | tf_op jit(solution)/shard_map/ppermute | solution.py:34
  146.5 0.9 copy-start.14
  157.1 4.4 %collective-permute-start.12 = (bf16[4,384,256]{2,1,0:T(8,128)(2,1)}, bf16[4,384,256]{2,1,0:T(8,128)(2,1)S(1)}, u32[]{:S(2)}, u32[]{:S(2)}) collective-permute-start(bf16[4,384,256]{2,1,0:T(8,128)(2,1)} %get-tuple-element.20), channel_id=1, source_target_pairs={{0,1},{1,0},{2,3},{3,2},{4,5},{5,4},{6,7},{7,6},{8,9},{9,8},{10,11... | collective-permute-start | bytes 2359304 | tf_op jit(solution)/shard_map/ppermute | solution.py:34
Sparse Core Ops, SparseCore 0:
  10.4 118.2 all-gather.1

commit v3 on v1

--- a/solution.py
+++ b/solution.py
@@ -92,6 +92,33 @@
 
 def halves(normed_ref, chip):
     return jnp.concatenate([normed_ref[chip, 0], normed_ref[chip, 1]], axis=1)
+
+
+def pack_kernel(rec_ref, mix_ref, scale_ref, out_hbm, both_ref, sems):
+    both_ref[0] = rec_ref[...].astype(BF16)
+    rows = mix_ref.shape[0]
+    scale = jnp.concatenate([scale_ref[...]] * (128 // rows), axis=1)
+    column = jnp.broadcast_to(scale, (128, 128)).T[:rows, :1]
+    both_ref[1] = (mix_ref[...] * column).astype(BF16)
+    copies = [
+        pltpu.make_async_copy(both_ref, out_hbm.at[i], sems.at[i]) for i in range(out_hbm.shape[0])
+    ]
+    for copy in copies:
+        copy.start()
+    for copy in copies:
+        copy.wait()
+
+
+def pack(rec, mix, scale, count):
+    rows, width = rec.shape
+    vmem = pl.BlockSpec(memory_space=pltpu.VMEM)
+    return pl.pallas_call(
+        pack_kernel,
+        out_shape=jax.ShapeDtypeStruct((count, 2, rows, width), BF16),
+        in_specs=[vmem] * 3,
+        out_specs=pl.BlockSpec(memory_space=pl.ANY),
+        scratch_shapes=[pltpu.VMEM((2, rows, width), BF16), pltpu.SemaphoreType.DMA((count,))],
+    )(rec, mix.T, scale.reshape(1, rows))
 
 
 def nearby(axis):
@@ -330,8 +357,6 @@
 ):
     rows, features = tokens.shape
     width = recurrent_input_weight.shape[1]
-    mix_rows = (mixing_output_weight * mixing_output_scale).T
-    pair = jnp.stack([recurrent_input_weight, mix_rows]).astype(BF16)
     down = (feedforward_down_weight * feedforward_down_scale).T
     half = down.shape[1] // 2
     ffn_blocks = over_plane(
@@ -339,12 +364,18 @@
         jnp.concatenate([feedforward_up_weight, down[:, half:]], axis=1),
     )
 
-    pair = copies_to(pair, "y")
+    copies = pack(
+        recurrent_input_weight, mixing_output_weight, mixing_output_scale, lax.axis_size("y")
+    )
+    pair = swap(copies, "y")
     rec_blocks = over_z(pair[:, 0].reshape(-1, width), 1)
     mix_blocks = over_z(pair[:, 1].reshape(-1, width), -1)
     rate = -DECAY_FACTOR * jax.nn.softplus(-channel_decay_parameter)
     count, size = recurrence_gate_weight_blocks.shape[:2]
-    tok = chips_from_here(tokens)
+    vectors = (recurrent_input_scale, rate, token_extra_log_decay)
+    vectors = [v.reshape(-1, 1, size) for v in vectors]
+    tok, scale, rate, extra = lax.optimization_barrier((tokens, *vectors))
+    tok = chips_from_here(tok)
     terms = [(4, rows, features)] * 2
     normed = pltpu.VMEM((4, 2, rows, features), BF16)
     (state,) = call(
@@ -354,12 +385,12 @@
             to_partner(tok),
             mixing_norm_gain.reshape(4, 2, 1, -1),
             *rec_blocks,
-            recurrent_input_scale.reshape(-1, 1, size),
+            scale,
             convolution_kernel_taps,
             recurrence_gate_weight_blocks,
             input_gate_weight_blocks,
-            rate.reshape(-1, 1, size),
-            token_extra_log_decay.reshape(-1, 1, size),
+            rate,
+            extra,
         ),
         (),
         [(rows, width)],

time: 186 us -> 186 us (level)
  Pallas kernels: 18.7 us -> 20.8 us
  other arithmetic: 8.34 us -> 6.47 us
    ppermute x6, waiting for transfers between devices: 17.4 us -> 19.9 us  [shift_z(): lax.ppermute(value, ('rep', 'z'), [(i, (i + step) % count) for i in range...]
    pallas_call x0 -> x1, Pallas kernels: none -> 2.11 us  [pack(): pl.pallas_call(pack_kernel, out_shape=jax.ShapeDtypeStruct((count, 2, row...]
    another operation x3 -> x0, other arithmetic: 1.93 us -> none  [layer(): pair = jnp.stack([recurrent_input_weight, mix_rows]).astype(BF16)]
  transfers between devices with their start and end apart: 15 -> 15, of which waited for: 9 -> 8; matrix products, arithmetic and copies ran while one was open for 5% -> 3% of each run, Pallas kernels for 5% -> 6%
where the time goes in v3:
time: 186 us; the launch traced here: 185 us
  starting transfers between devices  64.9 us (35%)
  blocking collectives  42.7 us (23%)
  waiting for transfers between devices  29.6 us (16%)
  Pallas kernels  20.8 us (11%)
  between operations  13.8 us (7%)
  other arithmetic  6.47 us (3%)
  local copies, waits for them, and re-layouts  6.31 us (3%)
    all_to_all x3, blocking collectives, swap(): return lax.all_to_all(value, axis, split_axis=0, concat_axis=0, tiled=True)  42.7 us
    ppermute x6, starting transfers between devices, shift_z(): lax.ppermute(value, ('rep', 'z'), [(i, (i + step) % count) for i in range...  27.8 us
    ppermute x6, waiting for transfers between devices, shift_z(): lax.ppermute(value, ('rep', 'z'), [(i, (i + step) % count) for i in range...  19.9 us
    ppermute x4, starting transfers between devices, to_partner(): return lax.ppermute(value, 'c', [(0, 1), (1, 0)])  19.5 us
    pallas_call x3, Pallas kernels, call(): pl.pallas_call(kernel, out_shape=[jax.ShapeDtypeStruct(shape, BF16) for s...  18.7 us
    ppermute x3, starting transfers between devices, shift_x(): lax.ppermute(value, 'x', [(i, (i + step) % count) for i in range(count)])  9.92 us
    all_to_all x1, starting transfers between devices, swap(): return lax.all_to_all(value, axis, split_axis=0, concat_axis=0, tiled=True)  7.65 us
    ppermute x4, waiting for transfers between devices, to_partner(): return lax.ppermute(value, 'c', [(0, 1), (1, 0)])  4.93 us
  transfers between devices with their start and end apart: 15, of which 8 were waited for; matrix products, arithmetic and copies ran while one was open for 3% of the time, Pallas kernels for 6%

profile of v3, /device:TPU:1, one launch (start us, length us, event | category | flops | bytes accessed | tf_op | source)
XLA Modules:
  0.0 184.6 jit_solution(10372175277501099174)
XLA Ops:
  6.5 1.0 multiply_bitcast_fusion
  7.5 0.1 fusion.3
  7.6 0.0 copy-start.13
  7.6 0.0 copy-start.11
  7.7 0.0 copy-start.12
  7.7 0.0 copy-start.4
  7.7 1.7 fusion
  9.4 0.0 all-gather.2.cloned.1.call-update
  9.4 2.1 %shard_map.172 = bf16[8,2,64,384]{3,2,1,0:T(8,128)(2,1)} custom-call(f32[64,384]{1,0:T(8,128)} %rec_ref.1, f32[64,384]{1,0:T(8,128)} %bitcast.22, f32[1,64]{1,0:T(1,128)} %bitcast.24), custom_call_target="tpu_custom_call" | custom-call | tf_op jit(solution)/shard_map/pallas_call | solution.py:115
  11.5 7.7 %all-to-all-start = ((bf16[8,2,64,384]{3,2,1,0:T(8,128)(2,1)}), bf16[8,2,64,384]{3,2,1,0:T(8,128)(2,1)S(1)}, u32[]{:S(2)}, u32[]{:S(2)}) async-start(bf16[8,2,64,384]{3,2,1,0:T(8,128)(2,1)} %shard_map.172), calls=%async_computation | async-start | bytes 1572864 | tf_op jit(solution)/shard_map/all_to_all | solution.py:26
  19.2 0.6 reshape.26.rate_ref
  19.8 0.6 reshape.25.scale_ref
  20.4 0.6 reshape.27.extra_ref
  21.0 3.1 %collective-permute-start = (bf16[384,256]{1,0:T(8,128)(2,1)S(1)}, bf16[384,256]{1,0:T(8,128)(2,1)S(1)}, u32[]{:S(2)}, u32[]{:S(2)}) collective-permute-start(bf16[384,256]{1,0:T(8,128)(2,1)S(1)} %copy-done.4), channel_id=1, source_target_pairs={{0,2},{2,4},{4,6},{6,0},{1,3},{3,5},{5,7},{7,1},{8,10},{10,12},{12... | collective-permute-start | bytes 589832 | tf_op jit(solution)/shard_map/ppermute | solution.py:43
  24.2 3.4 %collective-permute-start.1 = (bf16[384,256]{1,0:T(8,128)(2,1)S(1)}, bf16[384,256]{1,0:T(8,128)(2,1)S(1)}, u32[]{:S(2)}, u32[]{:S(2)}) collective-permute-start(bf16[384,256]{1,0:T(8,128)(2,1)S(1)} %copy-done.4), channel_id=1, source_target_pairs={{0,6},{2,0},{4,2},{6,4},{1,7},{3,1},{5,3},{7,5},{8,14},{10,8},{12,... | collective-permute-start | bytes 589832 | tf_op jit(solution)/shard_map/ppermute | solution.py:43
  27.5 3.4 %collective-permute-start.2 = (bf16[384,256]{1,0:T(8,128)(2,1)S(1)}, bf16[384,256]{1,0:T(8,128)(2,1)S(1)}, u32[]{:S(2)}, u32[]{:S(2)}) collective-permute-start(bf16[384,256]{1,0:T(8,128)(2,1)S(1)} %copy-done.4), channel_id=1, source_target_pairs={{0,4},{2,6},{4,0},{6,2},{1,5},{3,7},{5,1},{7,3},{8,12},{10,14},{12... | collective-permute-start | bytes 589832 | tf_op jit(solution)/shard_map/ppermute | solution.py:43
  31.0 0.0 collective-permute-done
  31.0 0.0 collective-permute-done.1
  31.0 4.7 %collective-permute-done.2 = bf16[384,256]{1,0:T(8,128)(2,1)S(1)} collective-permute-done((bf16[384,256]{1,0:T(8,128)(2,1)S(1)}, bf16[384,256]{1,0:T(8,128)(2,1)S(1)}, u32[]{:S(2)}, u32[]{:S(2)}) %collective-permute-start.2) | collective-permute-done | bytes 196640 | tf_op jit(solution)/shard_map/ppermute | solution.py:43
  35.8 0.1 pad_maximum_fusion.rows_ref
  35.9 6.1 %collective-permute-start.3 = (bf16[4,384,256]{2,1,0:T(8,128)(2,1)S(1)}, bf16[4,384,256]{2,1,0:T(8,128)(2,1)S(1)}, u32[]{:S(2)}, u32[]{:S(2)}) collective-permute-start(bf16[4,384,256]{2,1,0:T(8,128)(2,1)S(1)} %pad_maximum_fusion.rows_ref), channel_id=1, source_target_pairs={{0,1},{1,0},{2,3},{3,2},{4,5},{5,4},{6,7},{7,6},{8,9},{9,8},{10,11... | collective-permute-start | bytes 2359304 | tf_op jit(solution)/shard_map/ppermute | solution.py:34
  42.0 0.0 all-to-all-done
  42.0 0.1 fusion.2
  42.1 0.0 copy-start.1
  42.1 0.0 copy-start.8
  42.1 6.3 %collective-permute-start.4 = (bf16[512,384]{1,0:T(8,128)(2,1)S(1)}, bf16[512,384]{1,0:T(8,128)(2,1)S(1)}, u32[]{:S(2)}, u32[]{:S(2)}) collective-permute-start(bf16[512,384]{1,0:T(8,128)(2,1)S(1)} %bitcast.12), channel_id=1, source_target_pairs={{0,64},{64,128},{128,192},{192,256},{256,320},{320,384},{384,448},... | collective-permute-start | bytes 1179656 | tf_op jit(solution)/shard_map/ppermute | solution.py:22
  48.4 9.7 %collective-permute-start.8 = (bf16[512,384]{1,0:T(8,128)(2,1)S(1)}, bf16[512,384]{1,0:T(8,128)(2,1)S(1)}, u32[]{:S(2)}, u32[]{:S(2)}) collective-permute-start(bf16[512,384]{1,0:T(8,128)(2,1)S(1)} %bitcast.16), channel_id=1, source_target_pairs={{0,448},{64,0},{128,64},{192,128},{256,192},{320,256},{384,320},{4... | collective-permute-start | bytes 1179656 | tf_op jit(solution)/shard_map/ppermute | solution.py:22
  58.1 3.4 %collective-permute-start.5 = (bf16[512,384]{1,0:T(8,128)(2,1)S(1)}, bf16[512,384]{1,0:T(8,128)(2,1)S(1)}, u32[]{:S(2)}, u32[]{:S(2)}) collective-permute-start(bf16[512,384]{1,0:T(8,128)(2,1)S(1)} %bitcast.13), channel_id=1, source_target_pairs={{0,448},{64,0},{128,64},{192,128},{256,192},{320,256},{384,320},{4... | collective-permute-start | bytes 1179656 | tf_op jit(solution)/shard_map/ppermute | solution.py:22
  61.5 4.6 %collective-permute-done.4.before_ref = bf16[512,384]{1,0:T(8,128)(2,1)S(1)} collective-permute-done((bf16[512,384]{1,0:T(8,128)(2,1)S(1)}, bf16[512,384]{1,0:T(8,128)(2,1)S(1)}, u32[]{:S(2)}, u32[]{:S(2)}) %collective-permute-start.4) | collective-permute-done | bytes 393248 | tf_op jit(solution)/shard_map/ppermute | solution.py:22
  66.1 1.9 %collective-permute-start.6 = (bf16[512,384]{1,0:T(8,128)(2,1)S(1)}, bf16[512,384]{1,0:T(8,128)(2,1)S(1)}, u32[]{:S(2)}, u32[]{:S(2)}) collective-permute-start(bf16[512,384]{1,0:T(8,128)(2,1)S(1)} %collective-permute-done.4.before_ref), channel_id=1, source_target_pairs={{0,64},{64,128},{128,192},{192,256},{256,320},{320,384},{384,448},... | collective-permute-start | bytes 1179656 | tf_op jit(solution)/shard_map/ppermute | solution.py:22
  68.0 1.9 %collective-permute-start.7 = (bf16[512,384]{1,0:T(8,128)(2,1)S(1)}, bf16[512,384]{1,0:T(8,128)(2,1)S(1)}, u32[]{:S(2)}, u32[]{:S(2)}) collective-permute-start(bf16[512,384]{1,0:T(8,128)(2,1)S(1)} %bitcast.17), channel_id=1, source_target_pairs={{0,64},{64,128},{128,192},{192,256},{256,320},{320,384},{384,448},... | collective-permute-start | bytes 1179656 | tf_op jit(solution)/shard_map/ppermute | solution.py:22
  69.9 0.0 collective-permute-done.8.after_ref
  69.9 4.6 %collective-permute-start.9 = (bf16[512,384]{1,0:T(8,128)(2,1)S(1)}, bf16[512,384]{1,0:T(8,128)(2,1)S(1)}, u32[]{:S(2)}, u32[]{:S(2)}) collective-permute-start(bf16[512,384]{1,0:T(8,128)(2,1)S(1)} %collective-permute-done.8.after_ref), channel_id=1, source_target_pairs={{0,448},{64,0},{128,64},{192,128},{256,192},{320,256},{384,320},{4... | collective-permute-start | bytes 1179656 | tf_op jit(solution)/shard_map/ppermute | solution.py:22
  74.5 0.0 collective-permute-done.3.partner_ref
  74.5 1.0 collective-permute-done.5.after_ref
  75.6 4.2 %collective-permute-done.6.far_ref = bf16[512,384]{1,0:T(8,128)(2,1)S(1)} collective-permute-done((bf16[512,384]{1,0:T(8,128)(2,1)S(1)}, bf16[512,384]{1,0:T(8,128)(2,1)S(1)}, u32[]{:S(2)}, u32[]{:S(2)}) %collective-permute-start.6) | collective-permute-done | bytes 393248 | tf_op jit(solution)/shard_map/ppermute | solution.py:22
  79.8 0.7 copy-done.7
  80.5 6.0 %shard_map.173.state_ref = bf16[384,384]{1,0:T(8,128)(2,1)} custom-call(bf16[4,384,256]{2,1,0:T(8,128)(2,1)} %copy-done, bf16[4,384,256]{2,1,0:T(8,128)(2,1)} %copy-done.2, f32[4,2,1,256]{3,2,1,0:T(1,128)} %bitcast.23, bf16[512,384]{1,0:T(8,128)(2,1)} %bitcast.14, bf16[512,384]{1,0:T(8,128)(2,1)} %copy-done.5, bf16[512,384]{1,0:T(8,128)(2,1)} %copy-done.6, ...), custom_call_target="tpu_custom_call" | custom-call | flops 603979776 | tf_op jit(solution)/shard_map/pallas_call | solution.py:327
  86.5 10.1 %collective-permute-done.7.before_ref = bf16[512,384]{1,0:T(8,128)(2,1)S(1)} collective-permute-done((bf16[512,384]{1,0:T(8,128)(2,1)S(1)}, bf16[512,384]{1,0:T(8,128)(2,1)S(1)}, u32[]{:S(2)}, u32[]{:S(2)}) %collective-permute-start.7) | collective-permute-done | bytes 393248 | tf_op jit(solution)/shard_map/ppermute | solution.py:22
  96.6 0.0 collective-permute-done.9.far_ref
  96.6 0.7 copy-done.16
  97.3 0.7 copy-done.17
  98.1 3.3 %shard_map.174 = (bf16[4,384,256]{2,1,0:T(8,128)(2,1)}, bf16[4,384,256]{2,1,0:T(8,128)(2,1)}) custom-call(bf16[384,384]{1,0:T(8,128)(2,1)} %shard_map.173.state_ref, bf16[512,384]{1,0:T(8,128)(2,1)} %bitcast.18, bf16[512,384]{1,0:T(8,128)(2,1)} %copy-done.16, bf16[512,384]{1,0:T(8,128)(2,1)} %copy-done.15, bf16[512,384]{1,0:T(8,128)(2,1)} %copy-done.17), custom_call_target="tpu_custom_call" | custom-call | flops 603979776 | tf_op jit(solution)/shard_map/pallas_call | solution.py:327
  101.4 6.7 %collective-permute-start.10 = (bf16[4,384,256]{2,1,0:T(8,128)(2,1)}, bf16[4,384,256]{2,1,0:T(8,128)(2,1)S(1)}, u32[]{:S(2)}, u32[]{:S(2)}) collective-permute-start(bf16[4,384,256]{2,1,0:T(8,128)(2,1)} %get-tuple-element.18), channel_id=1, source_target_pairs={{0,1},{1,0},{2,3},{3,2},{4,5},{5,4},{6,7},{7,6},{8,9},{9,8},{10,11... | collective-permute-start | bytes 2359304 | tf_op jit(solution)/shard_map/ppermute | solution.py:34
  108.1 2.1 %collective-permute-done.10 = bf16[4,384,256]{2,1,0:T(8,128)(2,1)S(1)} collective-permute-done((bf16[4,384,256]{2,1,0:T(8,128)(2,1)}, bf16[4,384,256]{2,1,0:T(8,128)(2,1)S(1)}, u32[]{:S(2)}, u32[]{:S(2)}) %collective-permute-start.10) | collective-permute-done | bytes 786464 | tf_op jit(solution)/shard_map/ppermute | solution.py:34
  110.2 1.4 add_convert_fusion.1
  111.6 15.2 %all_to_all.20 = bf16[4,384,256]{2,1,0:T(8,128)(2,1)S(1)} all-to-all(bf16[4,384,256]{2,1,0:T(8,128)(2,1)S(1)} %add_convert_fusion.1), channel_id=1, replica_groups=mesh['rep'=2,'z'=4,'y'=8,'x'=4,'c'=2] {'x'}, dimensions={0} | all-to-all | bytes 1572864 | tf_op jit(solution)/shard_map/all_to_all | solution.py:26
  126.8 0.1 convert_reduce_fusion.1
  126.9 0.0 copy-start.9
  126.9 0.0 copy-start.10
  127.0 0.1 broadcast_in_dim.4
  127.0 13.1 %all_to_all.21.rows_ref = bf16[4,384,256]{2,1,0:T(8,128)(2,1)S(1)} all-to-all(bf16[4,384,256]{2,1,0:T(8,128)(2,1)S(1)} %broadcast_in_dim.4), channel_id=1, replica_groups=mesh['rep'=2,'z'=4,'y'=8,'x'=4,'c'=2] {'x'}, dimensions={0} | all-to-all | bytes 1572864 | tf_op jit(solution)/shard_map/all_to_all | solution.py:26
  140.1 4.5 %collective-permute-start.11 = (bf16[4,384,256]{2,1,0:T(8,128)(2,1)S(1)}, bf16[4,384,256]{2,1,0:T(8,128)(2,1)S(1)}, u32[]{:S(2)}, u32[]{:S(2)}) collective-permute-start(bf16[4,384,256]{2,1,0:T(8,128)(2,1)S(1)} %all_to_all.21.rows_ref), channel_id=1, source_target_pairs={{0,1},{1,0},{2,3},{3,2},{4,5},{5,4},{6,7},{7,6},{8,9},{9,8},{10,11... | collective-permute-start | bytes 2359304 | tf_op jit(solution)/shard_map/ppermute | solution.py:34
  144.6 0.6 reshape.31.gate_scale_ref
  145.2 0.5 reshape.32.up_scale_ref
  145.8 0.7 collective-permute-done.11.partner_ref
  146.5 0.9 copy-done.14
  147.4 9.4 %shard_map.175 = (bf16[4,384,256]{2,1,0:T(8,128)(2,1)}, bf16[4,384,256]{2,1,0:T(8,128)(2,1)}) custom-call(bf16[4,384,256]{2,1,0:T(8,128)(2,1)} %copy-done.3, bf16[4,384,256]{2,1,0:T(8,128)(2,1)} %copy-done.14, f32[4,2,1,256]{3,2,1,0:T(1,128)} %bitcast.25, f32[5,1,128]{2,1,0:T(1,128)} %reshape.31.gate_scale_ref, f32[5,1,128]{2,1,0:T(1,128)} %reshape.32.up_scale_ref, ...), custom_call_target="tpu_custom_call" | custom-call | flops 3019898880 | tf_op jit(solution)/shard_map/pallas_call | solution.py:327
  156.8 2.3 %collective-permute-start.12 = (bf16[4,384,256]{2,1,0:T(8,128)(2,1)}, bf16[4,384,256]{2,1,0:T(8,128)(2,1)S(1)}, u32[]{:S(2)}, u32[]{:S(2)}) collective-permute-start(bf16[4,384,256]{2,1,0:T(8,128)(2,1)} %get-tuple-element.20), channel_id=1, source_target_pairs={{0,1},{1,0},{2,3},{3,2},{4,5},{5,4},{6,7},{7,6},{8,9},{9,8},{10,11... | collective-permute-start | bytes 2359304 | tf_op jit(solution)/shard_map/ppermute | solution.py:34
  159.1 2.1 %collective-permute-done.12 = bf16[4,384,256]{2,1,0:T(8,128)(2,1)S(1)} collective-permute-done((bf16[4,384,256]{2,1,0:T(8,128)(2,1)}, bf16[4,384,256]{2,1,0:T(8,128)(2,1)S(1)}, u32[]{:S(2)}, u32[]{:S(2)}) %collective-permute-start.12) | collective-permute-done | bytes 786464 | tf_op jit(solution)/shard_map/ppermute | solution.py:34
  161.2 1.3 add_convert_fusion
  162.5 14.4 %all_to_all.22 = bf16[4,384,256]{2,1,0:T(8,128)(2,1)S(1)} all-to-all(bf16[4,384,256]{2,1,0:T(8,128)(2,1)S(1)} %add_convert_fusion), channel_id=1, replica_groups=mesh['rep'=2,'z'=4,'y'=8,'x'=4,'c'=2] {'x'}, dimensions={0} | all-to-all | bytes 1572864 | tf_op jit(solution)/shard_map/all_to_all | solution.py:26
  177.0 0.1 convert_reduce_fusion
  177.1 0.7 add_convert_fusion.2
  (28 shorter events, 0.1 us)
Async XLA Ops:
  6.5 140.0 %all-gather.2.cloned.1.call-start = ((), (), s32[]{:S(2)}) async-start(), calls=%async_computation.4 | async-start | bytes 8519680 | tf_op jit(solution)/shard_map/all_gather | solution.py:66
  7.6 11.6 %copy-start.13 = (f32[384]{0:T(512)S(1)}, f32[384]{0:T(512)}, u32[]{:S(2)}) copy-start(f32[384]{0:T(512)} %param.25) | copy-start | bytes 4612
  7.6 12.2 %copy-start.11 = (f32[384]{0:T(512)S(1)}, f32[384]{0:T(512)}, u32[]{:S(2)}) copy-start(f32[384]{0:T(512)} %param.21) | copy-start | bytes 4612
  7.7 12.8 %copy-start.12 = (f32[384]{0:T(512)S(1)}, f32[384]{0:T(512)}, u32[]{:S(2)}) copy-start(f32[384]{0:T(512)} %param.26) | copy-start | bytes 4612
  7.7 13.4 %copy-start.4 = (bf16[384,256]{1,0:T(8,128)(2,1)S(1)}, bf16[384,256]{1,0:T(8,128)(2,1)}, u32[]{:S(2)}) copy-start(bf16[384,256]{1,0:T(8,128)(2,1)} %param.18) | copy-start | bytes 589828
  11.5 30.4 %all-to-all-start = ((bf16[8,2,64,384]{3,2,1,0:T(8,128)(2,1)}), bf16[8,2,64,384]{3,2,1,0:T(8,128)(2,1)S(1)}, u32[]{:S(2)}, u32[]{:S(2)}) async-start(bf16[8,2,64,384]{3,2,1,0:T(8,128)(2,1)} %shard_map.172), calls=%async_computation | async-start | bytes 1572864 | tf_op jit(solution)/shard_map/all_to_all | solution.py:26
  21.0 9.9 %collective-permute-start = (bf16[384,256]{1,0:T(8,128)(2,1)S(1)}, bf16[384,256]{1,0:T(8,128)(2,1)S(1)}, u32[]{:S(2)}, u32[]{:S(2)}) collective-permute-start(bf16[384,256]{1,0:T(8,128)(2,1)S(1)} %copy-done.4), channel_id=1, source_target_pairs={{0,2},{2,4},{4,6},{6,0},{1,3},{3,5},{5,7},{7,1},{8,10},{10,12},{12... | collective-permute-start | bytes 589832 | tf_op jit(solution)/shard_map/ppermute | solution.py:43
  24.2 6.8 %collective-permute-start.1 = (bf16[384,256]{1,0:T(8,128)(2,1)S(1)}, bf16[384,256]{1,0:T(8,128)(2,1)S(1)}, u32[]{:S(2)}, u32[]{:S(2)}) collective-permute-start(bf16[384,256]{1,0:T(8,128)(2,1)S(1)} %copy-done.4), channel_id=1, source_target_pairs={{0,6},{2,0},{4,2},{6,4},{1,7},{3,1},{5,3},{7,5},{8,14},{10,8},{12,... | collective-permute-start | bytes 589832 | tf_op jit(solution)/shard_map/ppermute | solution.py:43
  27.5 8.2 %collective-permute-start.2 = (bf16[384,256]{1,0:T(8,128)(2,1)S(1)}, bf16[384,256]{1,0:T(8,128)(2,1)S(1)}, u32[]{:S(2)}, u32[]{:S(2)}) collective-permute-start(bf16[384,256]{1,0:T(8,128)(2,1)S(1)} %copy-done.4), channel_id=1, source_target_pairs={{0,4},{2,6},{4,0},{6,2},{1,5},{3,7},{5,1},{7,3},{8,12},{10,14},{12... | collective-permute-start | bytes 589832 | tf_op jit(solution)/shard_map/ppermute | solution.py:43
  35.9 43.9 %copy-start = (bf16[4,384,256]{2,1,0:T(8,128)(2,1)}, bf16[4,384,256]{2,1,0:T(8,128)(2,1)S(1)}, u32[]{:S(2)}) copy-start(bf16[4,384,256]{2,1,0:T(8,128)(2,1)S(1)} %pad_maximum_fusion.rows_ref) | copy-start | bytes 2359300
  35.9 38.7 %collective-permute-start.3 = (bf16[4,384,256]{2,1,0:T(8,128)(2,1)S(1)}, bf16[4,384,256]{2,1,0:T(8,128)(2,1)S(1)}, u32[]{:S(2)}, u32[]{:S(2)}) collective-permute-start(bf16[4,384,256]{2,1,0:T(8,128)(2,1)S(1)} %pad_maximum_fusion.rows_ref), channel_id=1, source_target_pairs={{0,1},{1,0},{2,3},{3,2},{4,5},{5,4},{6,7},{7,6},{8,9},{9,8},{10,11... | collective-permute-start | bytes 2359304 | tf_op jit(solution)/shard_map/ppermute | solution.py:34
  42.1 37.7 %copy-start.1 = (bf16[8,1,64,384]{3,2,1,0:T(8,128)(2,1)}, bf16[8,1,64,384]{3,2,1,0:T(8,128)(2,1)S(1)}, u32[]{:S(2)}) copy-start(bf16[8,1,64,384]{3,2,1,0:T(8,128)(2,1)S(1)} %get-tuple-element.22) | copy-start | bytes 1179652
  42.1 54.5 %copy-start.8 = (bf16[8,1,64,384]{3,2,1,0:T(8,128)(2,1)}, bf16[8,1,64,384]{3,2,1,0:T(8,128)(2,1)S(1)}, u32[]{:S(2)}) copy-start(bf16[8,1,64,384]{3,2,1,0:T(8,128)(2,1)S(1)} %get-tuple-element.21) | copy-start | bytes 1179652
  42.1 24.0 %collective-permute-start.4 = (bf16[512,384]{1,0:T(8,128)(2,1)S(1)}, bf16[512,384]{1,0:T(8,128)(2,1)S(1)}, u32[]{:S(2)}, u32[]{:S(2)}) collective-permute-start(bf16[512,384]{1,0:T(8,128)(2,1)S(1)} %bitcast.12), channel_id=1, source_target_pairs={{0,64},{64,128},{128,192},{192,256},{256,320},{320,384},{384,448},... | collective-permute-start | bytes 1179656 | tf_op jit(solution)/shard_map/ppermute | solution.py:22
  48.4 21.6 %collective-permute-start.8 = (bf16[512,384]{1,0:T(8,128)(2,1)S(1)}, bf16[512,384]{1,0:T(8,128)(2,1)S(1)}, u32[]{:S(2)}, u32[]{:S(2)}) collective-permute-start(bf16[512,384]{1,0:T(8,128)(2,1)S(1)} %bitcast.16), channel_id=1, source_target_pairs={{0,448},{64,0},{128,64},{192,128},{256,192},{320,256},{384,320},{4... | collective-permute-start | bytes 1179656 | tf_op jit(solution)/shard_map/ppermute | solution.py:22
  58.1 17.4 %collective-permute-start.5 = (bf16[512,384]{1,0:T(8,128)(2,1)S(1)}, bf16[512,384]{1,0:T(8,128)(2,1)S(1)}, u32[]{:S(2)}, u32[]{:S(2)}) collective-permute-start(bf16[512,384]{1,0:T(8,128)(2,1)S(1)} %bitcast.13), channel_id=1, source_target_pairs={{0,448},{64,0},{128,64},{192,128},{256,192},{320,256},{384,320},{4... | collective-permute-start | bytes 1179656 | tf_op jit(solution)/shard_map/ppermute | solution.py:22
  66.1 13.7 %copy-start.5 = (bf16[512,384]{1,0:T(8,128)(2,1)}, bf16[512,384]{1,0:T(8,128)(2,1)S(1)}, u32[]{:S(2)}) copy-start(bf16[512,384]{1,0:T(8,128)(2,1)S(1)} %collective-permute-done.4.before_ref) | copy-start | bytes 1179652
  66.1 13.7 %collective-permute-start.6 = (bf16[512,384]{1,0:T(8,128)(2,1)S(1)}, bf16[512,384]{1,0:T(8,128)(2,1)S(1)}, u32[]{:S(2)}, u32[]{:S(2)}) collective-permute-start(bf16[512,384]{1,0:T(8,128)(2,1)S(1)} %collective-permute-done.4.before_ref), channel_id=1, source_target_pairs={{0,64},{64,128},{128,192},{192,256},{256,320},{320,384},{384,448},... | collective-permute-start | bytes 1179656 | tf_op jit(solution)/shard_map/ppermute | solution.py:22
  68.0 28.6 %collective-permute-start.7 = (bf16[512,384]{1,0:T(8,128)(2,1)S(1)}, bf16[512,384]{1,0:T(8,128)(2,1)S(1)}, u32[]{:S(2)}, u32[]{:S(2)}) collective-permute-start(bf16[512,384]{1,0:T(8,128)(2,1)S(1)} %bitcast.17), channel_id=1, source_target_pairs={{0,64},{64,128},{128,192},{192,256},{256,320},{320,384},{384,448},... | collective-permute-start | bytes 1179656 | tf_op jit(solution)/shard_map/ppermute | solution.py:22
  69.9 26.7 %copy-start.15 = (bf16[512,384]{1,0:T(8,128)(2,1)}, bf16[512,384]{1,0:T(8,128)(2,1)S(1)}, u32[]{:S(2)}) copy-start(bf16[512,384]{1,0:T(8,128)(2,1)S(1)} %collective-permute-done.8.after_ref) | copy-start | bytes 1179652
  69.9 26.7 %collective-permute-start.9 = (bf16[512,384]{1,0:T(8,128)(2,1)S(1)}, bf16[512,384]{1,0:T(8,128)(2,1)S(1)}, u32[]{:S(2)}, u32[]{:S(2)}) collective-permute-start(bf16[512,384]{1,0:T(8,128)(2,1)S(1)} %collective-permute-done.8.after_ref), channel_id=1, source_target_pairs={{0,448},{64,0},{128,64},{192,128},{256,192},{320,256},{384,320},{4... | collective-permute-start | bytes 1179656 | tf_op jit(solution)/shard_map/ppermute | solution.py:22
  74.5 5.2 %copy-start.2 = (bf16[4,384,256]{2,1,0:T(8,128)(2,1)}, bf16[4,384,256]{2,1,0:T(8,128)(2,1)S(1)}, u32[]{:S(2)}) copy-start(bf16[4,384,256]{2,1,0:T(8,128)(2,1)S(1)} %collective-permute-done.3.partner_ref) | copy-start | bytes 2359300
  75.6 4.2 %copy-start.6 = (bf16[512,384]{1,0:T(8,128)(2,1)}, bf16[512,384]{1,0:T(8,128)(2,1)S(1)}, u32[]{:S(2)}) copy-start(bf16[512,384]{1,0:T(8,128)(2,1)S(1)} %collective-permute-done.5.after_ref) | copy-start | bytes 1179652
  79.8 0.8 copy-start.7
  96.6 0.7 copy-start.16
  97.3 0.7 copy-start.17
  101.4 8.8 %collective-permute-start.10 = (bf16[4,384,256]{2,1,0:T(8,128)(2,1)}, bf16[4,384,256]{2,1,0:T(8,128)(2,1)S(1)}, u32[]{:S(2)}, u32[]{:S(2)}) collective-permute-start(bf16[4,384,256]{2,1,0:T(8,128)(2,1)} %get-tuple-element.18), channel_id=1, source_target_pairs={{0,1},{1,0},{2,3},{3,2},{4,5},{5,4},{6,7},{7,6},{8,9},{9,8},{10,11... | collective-permute-start | bytes 2359304 | tf_op jit(solution)/shard_map/ppermute | solution.py:34
  126.9 17.7 %copy-start.9 = (f32[640]{0:T(1024)S(1)}, f32[640]{0:T(1024)}, u32[]{:S(2)}) copy-start(f32[640]{0:T(1024)} %param.31) | copy-start | bytes 7684
  126.9 18.3 %copy-start.10 = (f32[640]{0:T(1024)S(1)}, f32[640]{0:T(1024)}, u32[]{:S(2)}) copy-start(f32[640]{0:T(1024)} %param.33) | copy-start | bytes 7684
  140.1 6.4 %copy-start.3 = (bf16[4,384,256]{2,1,0:T(8,128)(2,1)}, bf16[4,384,256]{2,1,0:T(8,128)(2,1)S(1)}, u32[]{:S(2)}) copy-start(bf16[4,384,256]{2,1,0:T(8,128)(2,1)S(1)} %all_to_all.21.rows_ref) | copy-start | bytes 2359300
  140.1 6.4 %collective-permute-start.11 = (bf16[4,384,256]{2,1,0:T(8,128)(2,1)S(1)}, bf16[4,384,256]{2,1,0:T(8,128)(2,1)S(1)}, u32[]{:S(2)}, u32[]{:S(2)}) collective-permute-start(bf16[4,384,256]{2,1,0:T(8,128)(2,1)S(1)} %all_to_all.21.rows_ref), channel_id=1, source_target_pairs={{0,1},{1,0},{2,3},{3,2},{4,5},{5,4},{6,7},{7,6},{8,9},{9,8},{10,11... | collective-permute-start | bytes 2359304 | tf_op jit(solution)/shard_map/ppermute | solution.py:34
  146.5 0.9 copy-start.14
  156.8 4.4 %collective-permute-start.12 = (bf16[4,384,256]{2,1,0:T(8,128)(2,1)}, bf16[4,384,256]{2,1,0:T(8,128)(2,1)S(1)}, u32[]{:S(2)}, u32[]{:S(2)}) collective-permute-start(bf16[4,384,256]{2,1,0:T(8,128)(2,1)} %get-tuple-element.20), channel_id=1, source_target_pairs={{0,1},{1,0},{2,3},{3,2},{4,5},{5,4},{6,7},{7,6},{8,9},{9,8},{10,11... | collective-permute-start | bytes 2359304 | tf_op jit(solution)/shard_map/ppermute | solution.py:34
Sparse Core Ops, SparseCore 0:
  10.4 118.2 all-gather.1
